TPU v7x, 512 devices: a whole 4x4x16 slice. The times are simulated.
512 devices in a mesh: fs: 64 (over z, y), tp: 8 (over x, core).
Axes of the slice: x: 4, y: 4, z: 16, core: 2. Of those that a mesh axis runs over, the one named last changes fastest.
Arguments:
- residual_in: bfloat16 [16384, 2048], P(('fs', 'tp')), may hold values from -6 to 6
- gain_first: float32 [2048], replicated, may hold values from 0.1 to 1.9
- gain_mixer: float32 [2048], replicated, may hold values from 0.1 to 1.9
- gain_second: float32 [2048], replicated, may hold values from 0.1 to 1.9
- gate_weight: float32 [2048, 6144], P('fs', 'tp'), may hold values from -0.125 to 0.125
- gate_scale: float32 [6144], P('tp'), may hold values from 0.3 to 3
- up_weight: float32 [2048, 6144], P('fs', 'tp'), may hold values from -0.125 to 0.125
- up_scale: float32 [6144], P('tp'), may hold values from 0.3 to 3
- down_weight: float32 [6144, 2048], P('tp', 'fs'), may hold values from -0.078125 to 0.078125
- down_scale: float32 [2048], P('fs'), may hold values from 0.3 to 3
- query_weight: float32 [2048, 2048], P('fs', 'tp'), may hold values from -0.125 to 0.125
- query_scale: float32 [2048], P('tp'), may hold values from 0.3 to 3
- key_weight: float32 [2048, 2048], P('fs', 'tp'), may hold values from -0.125 to 0.125
- key_scale: float32 [2048], P('tp'), may hold values from 0.3 to 3
- value_weight: float32 [2048, 2048], P('fs', 'tp'), may hold values from -0.125 to 0.125
- value_scale: float32 [2048], P('tp'), may hold values from 0.3 to 3
- output_weight: float32 [2048, 2048], P('tp', 'fs'), may hold values from -0.125 to 0.125
- output_scale: float32 [2048], P('fs'), may hold values from 0.3 to 3
Outputs:
- residual_out: bfloat16 [16384, 2048], P(('fs', 'tp'))
All inputs are finite; a program needn't handle non-finite values.
Results may differ from a plain program's by a relative error of at most 0.028.
Values may be sent and summed in bfloat16 or wider, within the bound.
No kernel may reach another device: no remote copies, remote signals or barrier semaphores. Data moves between devices by JAX's collectives and lax.ppermute only.
A program may use at most 64 MiB of HBM per device.

v0:
```python
import jax
import jax.numpy as jnp
from jax import lax
from jax.experimental import pallas as pl
from jax.experimental.pallas import tpu as pltpu
from jax.sharding import Mesh
from jax.sharding import PartitionSpec as P


HEADS = 8
HEAD_DIM = 256
BLOCK = 64
TOK = 256
FS = ("z", "y")
TP = ("x", "c")
FS_TP = ("z", "y", "x", "c")


EPSILON = 1e-06
HEAD_FLOOR = 0.25
ROTARY_BASE = 10000.0
HIGHEST = lax.Precision.HIGHEST


def spread(own_rows):
    peers = lax.axis_size("x")
    sent = jnp.broadcast_to(own_rows[None], (peers, *own_rows.shape))
    return lax.all_to_all(sent, "x", 0, 0, tiled=True).reshape(-1, own_rows.shape[1])


def swapped(x):
    return lax.ppermute(x, "c", [(0, 1), (1, 0)])


def shifted(x, axis, by):
    peers = lax.axis_size(axis)
    return lax.ppermute(x, axis, [(i, (i + by) % peers) for i in range(peers)])


def after(x, first):
    return lax.optimization_barrier((x, first))[0]


def y_neighbours(part):
    return shifted(part, "y", 1), shifted(part, "y", -1)


def y_opposite(below, above):
    half = below.shape[0] // 2
    return shifted(below[:half], "y", 1), shifted(above[half:], "y", -1)


def joined_over_y(part, below, above, far):
    me, peers = lax.axis_index("y"), lax.axis_size("y")
    own = part[:, :, None]
    whole = jnp.broadcast_to(own, (*part.shape[:2], peers, *part.shape[2:]))
    for piece, by in ((below, 3), (far, 2), (above, 1)):
        place = (0, 0, (me + by) % peers, 0, 0)
        whole = lax.dynamic_update_slice(whole, piece[:, :, None], place)
    return whole.reshape(part.shape[0], -1, part.shape[3])


def prepare_kernel(
    gate_ref, up_ref, down_ref, down_scale_ref, query_ref, key_ref, value_ref, output_ref, output_scale_ref,
    first_ref, second_ref, third_ref,
):
    low = jnp.bfloat16
    rows, hidden_width = gate_ref.shape
    width = query_ref.shape[1]
    first_ref[:, :hidden_width] = gate_ref[...].astype(low)
    first_ref[:, hidden_width : 2 * hidden_width] = up_ref[...].astype(low)
    first_ref[:, 2 * hidden_width :] = jnp.zeros((rows, width), low)
    second_ref[...] = scaled_rows(down_ref[...], down_scale_ref[...])
    for k, ref in enumerate((query_ref, key_ref, value_ref)):
        third_ref[pl.ds(k * rows, rows), :] = ref[...].astype(low)
    third_ref[pl.ds(3 * rows, rows), :] = scaled_rows(output_ref[...], output_scale_ref[...])


def scaled_rows(turned, factor):
    low = turned.astype(jnp.bfloat16).astype(jnp.float32)
    column = jnp.broadcast_to(factor, (8, factor.shape[1])).T[:, :1]
    return (low * column).astype(jnp.bfloat16)


def prepare(gate, up, down, down_scale, query, key, value, output, output_scale):
    rows, hidden_width = gate.shape
    width = query.shape[1]
    shapes = ((rows, 2 * hidden_width + width), (rows, hidden_width), (4 * rows, width))
    return pl.pallas_call(
        prepare_kernel,
        out_shape=[jax.ShapeDtypeStruct(x, jnp.bfloat16) for x in shapes],
        cost_estimate=pl.CostEstimate(
            flops=rows * (3 * hidden_width + 4 * width),
            bytes_accessed=6 * rows * (3 * hidden_width + 4 * width),
            transcendentals=0,
        ),
    )(
        gate, up, down.T, down_scale[None], query, key, value, output.T, output_scale[None]
    )


def normalize(sequence_rows, gain_vector):
    values = sequence_rows.astype(jnp.float32)
    scaled = values * lax.rsqrt(jnp.mean(values * values, axis=-1, keepdims=True) + EPSILON)
    return (scaled * gain_vector).astype(jnp.bfloat16)


def collect_rows(own_rows, gain_vector):
    near = spread(normalize(own_rows, gain_vector))
    return near, swapped(near)


def product(inputs, turned):
    return lax.dot_general(
        inputs, turned, (((1,), (1,)), ((), ())), preferred_element_type=jnp.float32
    )


def return_rows(near, far):
    pair = near.astype(jnp.float32) + swapped(far).astype(jnp.float32)
    pieces = pair.astype(jnp.bfloat16).reshape(lax.axis_size("x"), -1, near.shape[1])
    arrived = lax.all_to_all(pieces, "x", 0, 0, tiled=True)
    return arrived.astype(jnp.float32).sum(axis=0)


def head_rates(first_head, head_count, length):
    head_number = (first_head + jnp.arange(head_count)).astype(jnp.float32)
    return jnp.exp(jnp.log(1.0 / 16.0) + head_number / (HEADS - 1) * jnp.log(4.0 / length))


VMEM = pl.BlockSpec(memory_space=pltpu.VMEM)
KERNEL_PARAMS = pltpu.CompilerParams(vmem_limit_bytes=20 * 1024 * 1024)


def mlp_kernel(near_ref, far_ref, gate_up, down, gate_scale, up_scale, out_near, out_far):
    half, width = near_ref.shape
    units, tile = down.shape[1], 256
    x = jnp.concatenate([near_ref[...], far_ref[...]], axis=0)
    hidden = []
    for first in range(0, units, tile):
        here, there = pl.ds(first, tile), pl.ds(units + first, tile)
        gate = jnp.dot(x, gate_up[:, here], preferred_element_type=jnp.float32)
        up = jnp.dot(x, gate_up[:, there], preferred_element_type=jnp.float32)
        gate, up = gate * gate_scale[:, here], up * up_scale[:, here]
        hidden.append((gate / (1.0 + jnp.exp(-gate)) * up).astype(jnp.bfloat16))
    hidden = jnp.concatenate(hidden, axis=1)
    for first in range(0, width, 512):
        here = pl.ds(first, 512)
        term = product(hidden, down[here, :]).astype(jnp.bfloat16)
        out_near[:, here] = term[:half, :]
        out_far[:, here] = term[half:, :]


def mlp(near, far, gate_up, down_turned, gate_scale, up_scale):
    half, width = near.shape
    units = gate_scale.shape[0]
    return pl.pallas_call(
        mlp_kernel,
        in_specs=[VMEM] * 6,
        out_specs=[VMEM] * 2,
        out_shape=[jax.ShapeDtypeStruct((half, width), jnp.bfloat16)] * 2,
        compiler_params=KERNEL_PARAMS,
        cost_estimate=pl.CostEstimate(
            flops=12 * half * width * units,
            bytes_accessed=6 * width * units + 8 * half * width,
            transcendentals=2 * half * units,
        ),
    )(near, far, gate_up, down_turned, gate_scale[None], up_scale[None])


def mixer_kernel(
    place_ref, near_ref, far_ref, own_ref, below_ref, above_ref, beyond_ref, scale_ref,
    cosine_ref, sine_ref, within_ref, fading_ref, rising_ref, decay_ref, out_near_ref, out_far_ref,
    both, weight, query, key, value, mixed, sorted_,
):
    half = near_ref.shape[0]
    rows = half // 4
    core, y = place_ref[0], place_ref[1]

    def place_of(part, number):
        return pl.ds(pl.multiple_of(part * 2 * rows + number * rows, rows), rows)

    def whole_weight(k):
        for piece_ref, by in ((own_ref, 0), (below_ref, 3), (above_ref, 1), (beyond_ref, 2)):
            weight[k, :, lax.rem(y + by, 4), :, :] = piece_ref[:, k]
        return weight[k].reshape(-1, HEAD_DIM)

    for part in range(4):
        here = pl.ds(part * rows, rows)
        both[place_of(part, core), :] = near_ref[here, :]
        both[place_of(part, 1 - core), :] = far_ref[here, :]

    def projected(k):
        pre = jnp.dot(both[...], whole_weight(k), preferred_element_type=jnp.float32)
        return pre * scale_ref[:, k * HEAD_DIM : (k + 1) * HEAD_DIM]

    def turned(values):
        middle = HEAD_DIM // 2
        a, b = values[:, :middle], values[:, middle:]
        cosine, sine = cosine_ref[...], sine_ref[...]
        return jnp.concatenate([a * cosine - b * sine, b * cosine + a * sine], axis=1)

    query[...] = turned(projected(0)).astype(jnp.bfloat16)
    key[...] = turned(projected(1)).astype(jnp.bfloat16)
    value[...] = projected(2).astype(jnp.bfloat16)
    blocks = query.shape[0] // BLOCK
    state = None
    for n in range(blocks):
        place = pl.ds(n * BLOCK, BLOCK)
        q, k, v = query[place, :], key[place, :], value[place, :]
        weights = (product(q, k) * within_ref[...]).astype(jnp.bfloat16)
        combined = jnp.dot(weights, v, preferred_element_type=jnp.float32)
        if n > 0:
            queried = q.astype(jnp.float32) * rising_ref[...]
            combined += jnp.dot(
                queried, state, precision=HIGHEST, preferred_element_type=jnp.float32
            )
        if n < blocks - 1:
            faded = (k.astype(jnp.float32) * fading_ref[...]).T
            update = jnp.dot(
                faded,
                v.astype(jnp.float32),
                precision=HIGHEST,
                preferred_element_type=jnp.float32,
            )
            state = update if n == 0 else state * decay_ref[...] + update
        square = jnp.mean(combined * combined, axis=1, keepdims=True)
        normed = combined * lax.rsqrt(jnp.maximum(square, HEAD_FLOOR))
        mixed[place, :] = normed.astype(jnp.bfloat16)
    for part in range(4):
        here, there = pl.ds(part * rows, rows), pl.ds(half + part * rows, rows)
        sorted_[here, :] = mixed[place_of(part, core), :]
        sorted_[there, :] = mixed[place_of(part, 1 - core), :]
    output = whole_weight(3)
    for first in range(0, output.shape[0], 512):
        here = pl.ds(first, 512)
        term = product(sorted_[...], output[first : first + 512, :]).astype(jnp.bfloat16)
        out_near_ref[:, here] = term[:half, :]
        out_far_ref[:, here] = term[half:, :]


def mixer_tables(rows, rate):
    positions = jnp.arange(rows, dtype=jnp.float32)
    half = HEAD_DIM // 2
    frequency = ROTARY_BASE ** (-jnp.arange(half, dtype=jnp.float32) * 2.0 / HEAD_DIM)
    angles = positions[:, None] * frequency[None, :]
    inside = jnp.arange(BLOCK, dtype=jnp.float32)
    distance = inside[:, None] - inside[None, :]
    within = jnp.where(distance >= 0, jnp.exp(-rate * jnp.maximum(distance, 0.0)), 0.0)
    fading = jnp.exp(-rate * (BLOCK - 1.0 - inside[:, None])) * HEAD_DIM ** (-0.5)
    rising = jnp.exp(-rate * (inside[:, None] + 1.0))
    return (
        jnp.cos(angles),
        jnp.sin(angles),
        within * HEAD_DIM ** (-0.5),
        jnp.broadcast_to(fading, (BLOCK, HEAD_DIM)),
        jnp.broadcast_to(rising, (BLOCK, HEAD_DIM)),
        jnp.broadcast_to(jnp.exp(-rate * BLOCK), (1, HEAD_DIM)),
    )


def mixer(near, far, pieces, scales, tables, place):
    half_rows, width = near.shape
    rows = 2 * half_rows
    return pl.pallas_call(
        mixer_kernel,
        in_specs=[
            pl.BlockSpec(memory_space=pltpu.SMEM),
            *[VMEM] * (3 + len(pieces) + len(tables)),
        ],
        out_specs=[VMEM] * 2,
        out_shape=[jax.ShapeDtypeStruct((half_rows, width), jnp.bfloat16)] * 2,
        scratch_shapes=[
            pltpu.VMEM((rows, width), jnp.bfloat16),
            pltpu.VMEM((4, pieces[0].shape[0], 4, *pieces[0].shape[2:]), jnp.bfloat16),
            *[pltpu.VMEM((rows, HEAD_DIM), jnp.bfloat16) for _ in range(5)],
        ],
        compiler_params=KERNEL_PARAMS,
        cost_estimate=pl.CostEstimate(
            flops=10 * rows * width * HEAD_DIM,
            bytes_accessed=8 * width * HEAD_DIM + 4 * rows * width,
            transcendentals=rows,
        ),
    )(place, near, far, *pieces, scales[None], *tables)


def layer(
    residual_in,
    gain_first,
    gain_mixer,
    gain_second,
    gate_weight,
    gate_scale,
    up_weight,
    up_scale,
    down_weight,
    down_scale,
    query_weight,
    query_scale,
    key_weight,
    key_scale,
    value_weight,
    value_scale,
    output_weight,
    output_scale,
):
    low = jnp.bfloat16
    z, rows = lax.axis_size("z"), gate_weight.shape[0]
    hidden_width, local_width = down_weight.shape[0], query_weight.shape[1]
    packed, second_part, third_part = prepare(
        gate_weight, up_weight, down_weight, down_scale, query_weight, key_weight, value_weight,
        output_weight, output_scale,
    )
    packed_y = lax.all_gather(packed, "y", axis=0, tiled=True)
    packed_y = lax.dynamic_update_slice(packed_y, third_part, (0, 2 * hidden_width))
    whole_z = lax.all_gather(packed_y, "z", axis=0, tiled=True)
    second_z = lax.all_gather(after(second_part, packed_y), "z", axis=0, tiled=True)
    second_near = y_neighbours(second_z)
    first_rows = collect_rows(after(residual_in, second_z), gain_first)
    second_far = y_opposite(*second_near)
    down_full = joined_over_y(
        *[
            x.reshape(1, z, rows, hidden_width)
            for x in (second_z, *second_near, jnp.concatenate(second_far, axis=0))
        ]
    )[0]
    third_z = whole_z[:, 2 * hidden_width :]
    third_below = shifted(third_z, "y", 1)
    third_above = shifted(third_z, "y", -1)
    third_far = shifted(third_below, "y", 1)
    core = lax.axis_index("c")
    rate = head_rates(lax.axis_index("x") * lax.axis_size("c") + core, 1, TOK)[0]
    scales = jnp.concatenate([query_scale, key_scale, value_scale])
    place = jnp.stack([core, lax.axis_index("y")]).astype(jnp.int32)
    first_rows, scales, place = lax.optimization_barrier((first_rows, scales, place))
    first_term = mlp(*first_rows, whole_z, down_full, gate_scale, up_scale)
    tables = mixer_tables(TOK, rate)
    mlp_first = return_rows(*first_term)
    pieces = [
        x.reshape(-1, 4, rows, local_width)
        for x in (third_z, third_below, third_above, third_far)
    ]
    middle = (residual_in.astype(jnp.float32) + 0.5 * mlp_first).astype(low)
    mixer_rows = collect_rows(middle, gain_mixer)
    mixer_term = mixer(*mixer_rows, pieces, scales, tables, place)
    second = (middle.astype(jnp.float32) + return_rows(*mixer_term)).astype(low)
    second_rows = collect_rows(second, gain_second)
    mlp_second = return_rows(*mlp(*second_rows, whole_z, down_full, gate_scale, up_scale))
    return (second.astype(jnp.float32) + 0.5 * mlp_second).astype(low)


def solution(mesh):
    split = Mesh(mesh.devices.reshape(16, 4, 4, 2), FS_TP)
    in_specs = (
        P(FS_TP, None),
        P(),
        P(),
        P(),
        P(FS, TP),
        P(TP),
        P(FS, TP),
        P(TP),
        P(TP, FS),
        P(FS),
        P(FS, TP),
        P(TP),
        P(FS, TP),
        P(TP),
        P(FS, TP),
        P(TP),
        P(TP, FS),
        P(FS),
    )
    out_specs = P(FS_TP, None)
    return jax.shard_map(layer, mesh=split, in_specs=in_specs, out_specs=out_specs, check_vma=False)
```

profile of v0, /device:TPU:1, one launch (start us, length us, event | category | flops | bytes accessed | tf_op | source)
XLA Modules:
  0.0 260.9 jit_solution(15703274548889773381)
XLA Ops:
  8.5 11.3 %all_gather.9 = bf16[128,1792]{1,0:T(8,128)(2,1)S(1)} all-gather(bf16[32,1792]{1,0:T(8,128)(2,1)} %get-tuple-element.21), channel_id=1, replica_groups=mesh['z'=16,'y'=4,'x'=4,'c'=2] {'y'}, dimensions={0}, use_global_device_ids=true | all-gather | bytes 573440 | tf_op jit(solution)/shard_map/all_gather | solution.py:314
  21.4 38.5 %all_gather.10 = bf16[512,768]{1,0:T(8,128)(2,1)S(1)} all-gather(bf16[32,768]{1,0:T(8,128)(2,1)} %get-tuple-element.23), channel_id=1, replica_groups=mesh['z'=16,'y'=4,'x'=4,'c'=2] {'z'}, dimensions={0}, use_global_device_ids=true | all-gather | bytes 835584 | tf_op jit(solution)/shard_map/all_gather | solution.py:317
  59.9 1.9 collective-permute-start.1
  61.8 4.6 %collective-permute-start.3 = (bf16[512,768]{1,0:T(8,128)(2,1)S(1)}, bf16[512,768]{1,0:T(8,128)(2,1)S(1)}, u32[]{:S(2)}, u32[]{:S(2)}) collective-permute-start(bf16[512,768]{1,0:T(8,128)(2,1)S(1)} %all_gather.10), channel_id=1, source_target_pairs={{0,24},{8,0},{16,8},{24,16},{1,25},{9,1},{17,9},{25,17},{2,26},{10... | collective-permute-start | bytes 2359304 | tf_op jit(solution)/shard_map/ppermute | solution.py:37
  68.5 12.5 %all_to_all.30 = bf16[4,32,2048]{2,1,0:T(8,128)(2,1)} all-to-all(bf16[4,32,2048]{2,1,0:T(8,128)(2,1)S(1)} %broadcast_in_dim.30), channel_id=1, replica_groups=mesh['z'=16,'y'=4,'x'=4,'c'=2] {'x'}, dimensions={0} | all-to-all | bytes 1048576 | tf_op jit(solution)/shard_map/all_to_all | solution.py:28
  81.0 11.8 %collective-permute-start = (bf16[128,2048]{1,0:T(8,128)(2,1)}, bf16[128,2048]{1,0:T(8,128)(2,1)}, u32[]{:S(2)}, u32[]{:S(2)}) collective-permute-start(bf16[128,2048]{1,0:T(8,128)(2,1)} %bitcast.4.near_ref), channel_id=1, source_target_pairs={{0,1},{1,0},{2,3},{3,2},{4,5},{5,4},{6,7},{7,6},{8,9},{9,8},{10,11... | collective-permute-start | bytes 1572872 | tf_op jit(solution)/shard_map/ppermute | solution.py:32
  93.0 2.5 collective-permute-start.2
  97.2 4.0 %collective-permute-start.4 = (bf16[256,768]{1,0:T(8,128)(2,1)}, bf16[256,768]{1,0:T(8,128)(2,1)}, u32[]{:S(2)}, u32[]{:S(2)}) collective-permute-start(bf16[256,768]{1,0:T(8,128)(2,1)} %slice.13), channel_id=1, source_target_pairs={{0,24},{8,0},{16,8},{24,16},{1,25},{9,1},{17,9},{25,17},{2,26},{10... | collective-permute-start | bytes 1179656 | tf_op jit(solution)/shard_map/ppermute | solution.py:37
  103.2 3.6 %collective-permute-done.2 = bf16[256,768]{1,0:T(8,128)(2,1)} collective-permute-done((bf16[256,768]{1,0:T(8,128)(2,1)S(1)}, bf16[256,768]{1,0:T(8,128)(2,1)}, u32[]{:S(2)}, u32[]{:S(2)}) %collective-permute-start.2) | collective-permute-done | bytes 393248 | tf_op jit(solution)/shard_map/ppermute | solution.py:37
  106.8 3.0 %collective-permute-done.4 = bf16[256,768]{1,0:T(8,128)(2,1)} collective-permute-done((bf16[256,768]{1,0:T(8,128)(2,1)}, bf16[256,768]{1,0:T(8,128)(2,1)}, u32[]{:S(2)}, u32[]{:S(2)}) %collective-permute-start.4) | collective-permute-done | bytes 393248 | tf_op jit(solution)/shard_map/ppermute | solution.py:37
  111.1 16.5 %all-gather.2.cloned.1.call-done.gate_up = bf16[2048,1792]{1,0:T(8,128)(2,1)} async-done(((bf16[128,1792]{1,0:T(8,128)(2,1)}), bf16[2048,1792]{1,0:T(8,128)(2,1)}) %all-gather.2.cloned.1.call-update) | async-done | bytes 7340048 | tf_op jit(solution)/shard_map/all_gather | solution.py:316
  127.7 3.1 %copy-done = bf16[2048,1792]{1,0:T(8,128)(2,1)S(1)} copy-done((bf16[2048,1792]{1,0:T(8,128)(2,1)S(1)}, bf16[2048,1792]{1,0:T(8,128)(2,1)}, u32[]{:S(2)}) %copy-start) | copy-done | bytes 7340056
  130.8 3.8 %shard_map.173 = (bf16[128,2048]{1,0:T(8,128)(2,1)S(1)}, bf16[128,2048]{1,0:T(8,128)(2,1)S(1)}) custom-call(bf16[128,2048]{1,0:T(8,128)(2,1)} %bitcast.4.near_ref, bf16[128,2048]{1,0:T(8,128)(2,1)} %collective-permute-done.far_ref, bf16[2048,1792]{1,0:T(8,128)(2,1)S(1)} %copy-done, bf16[2048,768]{1,0:T(8,128)(2,1)S(1)} %bitcast.29, ...), custom_call_target="tpu_custom_call" | custom-call | flops 2415919104 | bytes 11534336 | tf_op jit(solution)/shard_map/pallas_call | solution.py:157
  134.6 2.9 %collective-permute-start.5 = (bf16[128,2048]{1,0:T(8,128)(2,1)S(1)}, bf16[128,2048]{1,0:T(8,128)(2,1)S(1)}, u32[]{:S(2)}, u32[]{:S(2)}) collective-permute-start(bf16[128,2048]{1,0:T(8,128)(2,1)S(1)} %get-tuple-element.28), channel_id=1, source_target_pairs={{0,1},{1,0},{2,3},{3,2},{4,5},{5,4},{6,7},{7,6},{8,9},{9,8},{10,11... | collective-permute-start | bytes 1572872 | tf_op jit(solution)/shard_map/ppermute | solution.py:32
  138.5 3.1 %collective-permute-start.7 = (bf16[2048,256]{1,0:T(8,128)(2,1)}, bf16[2048,256]{1,0:T(8,128)(2,1)}, u32[]{:S(2)}, u32[]{:S(2)}) collective-permute-start(bf16[2048,256]{1,0:T(8,128)(2,1)} %slice.14), channel_id=1, source_target_pairs={{0,8},{8,16},{16,24},{24,0},{1,9},{9,17},{17,25},{25,1},{2,10},{10... | collective-permute-start | bytes 3145736 | tf_op jit(solution)/shard_map/ppermute | solution.py:37
  142.6 4.0 %all-to-all-start.1 = ((bf16[4,32,2048]{2,1,0:T(8,128)(2,1)}), bf16[4,32,2048]{2,1,0:T(8,128)(2,1)S(1)}, u32[]{:S(2)}, u32[]{:S(2)}) async-start(bf16[4,32,2048]{2,1,0:T(8,128)(2,1)} %bitcast.15), calls=%async_computation.1 | async-start | bytes 1048576 | tf_op jit(solution)/shard_map/all_to_all | solution.py:122
  146.5 3.4 %collective-permute-start.8 = (bf16[2048,256]{1,0:T(8,128)(2,1)}, bf16[2048,256]{1,0:T(8,128)(2,1)}, u32[]{:S(2)}, u32[]{:S(2)}) collective-permute-start(bf16[2048,256]{1,0:T(8,128)(2,1)} %slice.14), channel_id=1, source_target_pairs={{0,24},{8,0},{16,8},{24,16},{1,25},{9,1},{17,9},{25,17},{2,26},{10... | collective-permute-start | bytes 3145736 | tf_op jit(solution)/shard_map/ppermute | solution.py:37
  149.9 5.6 %all-to-all-done.1 = bf16[4,32,2048]{2,1,0:T(8,128)(2,1)S(1)} async-done(((bf16[4,32,2048]{2,1,0:T(8,128)(2,1)}), bf16[4,32,2048]{2,1,0:T(8,128)(2,1)S(1)}, u32[]{:S(2)}, u32[]{:S(2)}) %all-to-all-start.1) | async-done | bytes 524320 | tf_op jit(solution)/shard_map/all_to_all | solution.py:122
  155.8 10.8 %collective-permute-done.7 = bf16[2048,256]{1,0:T(8,128)(2,1)} collective-permute-done((bf16[2048,256]{1,0:T(8,128)(2,1)}, bf16[2048,256]{1,0:T(8,128)(2,1)}, u32[]{:S(2)}, u32[]{:S(2)}) %collective-permute-start.7) | collective-permute-done | bytes 1048608 | tf_op jit(solution)/shard_map/ppermute | solution.py:37
  166.6 1.9 collective-permute-start.9
  169.5 4.3 %all-to-all-start.2 = ((bf16[4,32,2048]{2,1,0:T(8,128)(2,1)}), bf16[4,32,2048]{2,1,0:T(8,128)(2,1)}, u32[]{:S(2)}, u32[]{:S(2)}) async-start(bf16[4,32,2048]{2,1,0:T(8,128)(2,1)} %broadcast_in_dim.35), calls=%async_computation.2 | async-start | bytes 1048576 | tf_op jit(solution)/shard_map/all_to_all | solution.py:28
  173.9 8.0 %all-to-all-done.2 = bf16[4,32,2048]{2,1,0:T(8,128)(2,1)} async-done(((bf16[4,32,2048]{2,1,0:T(8,128)(2,1)}), bf16[4,32,2048]{2,1,0:T(8,128)(2,1)}, u32[]{:S(2)}, u32[]{:S(2)}) %all-to-all-start.2) | async-done | bytes 524320 | tf_op jit(solution)/shard_map/all_to_all | solution.py:28
  181.9 4.3 %collective-permute-start.6 = (bf16[128,2048]{1,0:T(8,128)(2,1)}, bf16[128,2048]{1,0:T(8,128)(2,1)S(1)}, u32[]{:S(2)}, u32[]{:S(2)}) collective-permute-start(bf16[128,2048]{1,0:T(8,128)(2,1)} %bitcast.16.near_ref), channel_id=1, source_target_pairs={{0,1},{1,0},{2,3},{3,2},{4,5},{5,4},{6,7},{7,6},{8,9},{9,8},{10,11... | collective-permute-start | bytes 1572872 | tf_op jit(solution)/shard_map/ppermute | solution.py:32
  187.9 6.0 %collective-permute-done.9 = bf16[2048,256]{1,0:T(8,128)(2,1)} collective-permute-done((bf16[2048,256]{1,0:T(8,128)(2,1)}, bf16[2048,256]{1,0:T(8,128)(2,1)}, u32[]{:S(2)}, u32[]{:S(2)}) %collective-permute-start.9) | collective-permute-done | bytes 1048608 | tf_op jit(solution)/shard_map/ppermute | solution.py:37
  194.1 6.4 %shard_map.174 = (bf16[128,2048]{1,0:T(8,128)(2,1)S(1)}, bf16[128,2048]{1,0:T(8,128)(2,1)S(1)}) custom-call(s32[2]{0:T(128)S(1)} %pad_add_fusion.place_ref, bf16[128,2048]{1,0:T(8,128)(2,1)} %bitcast.16.near_ref, bf16[128,2048]{1,0:T(8,128)(2,1)S(1)} %collective-permute-done.6.far_ref, bf16[16,4,32,256]{3,2,1,0:T(8,128)(2,1)} %bitcast.17.own_ref, ...), custom_call_target="tpu_custom_call" | custom-call | flops 1342177280 | bytes 6291456 | tf_op jit(solution)/shard_map/pallas_call | solution.py:265
  200.4 3.9 %collective-permute-start.10 = (bf16[128,2048]{1,0:T(8,128)(2,1)S(1)}, bf16[128,2048]{1,0:T(8,128)(2,1)S(1)}, u32[]{:S(2)}, u32[]{:S(2)}) collective-permute-start(bf16[128,2048]{1,0:T(8,128)(2,1)S(1)} %get-tuple-element.32), channel_id=1, source_target_pairs={{0,1},{1,0},{2,3},{3,2},{4,5},{5,4},{6,7},{7,6},{8,9},{9,8},{10,11... | collective-permute-start | bytes 1572872 | tf_op jit(solution)/shard_map/ppermute | solution.py:32
  206.0 12.4 %all_to_all.31 = bf16[4,32,2048]{2,1,0:T(8,128)(2,1)S(1)} all-to-all(bf16[4,32,2048]{2,1,0:T(8,128)(2,1)S(1)} %bitcast.35), channel_id=1, replica_groups=mesh['z'=16,'y'=4,'x'=4,'c'=2] {'x'}, dimensions={0} | all-to-all | bytes 1048576 | tf_op jit(solution)/shard_map/all_to_all | solution.py:122
  218.8 10.2 %all_to_all.32 = bf16[4,32,2048]{2,1,0:T(8,128)(2,1)S(1)} all-to-all(bf16[4,32,2048]{2,1,0:T(8,128)(2,1)S(1)} %broadcast_in_dim.40), channel_id=1, replica_groups=mesh['z'=16,'y'=4,'x'=4,'c'=2] {'x'}, dimensions={0} | all-to-all | bytes 1048576 | tf_op jit(solution)/shard_map/all_to_all | solution.py:28
  229.0 4.7 %collective-permute-start.11 = (bf16[128,2048]{1,0:T(8,128)(2,1)S(1)}, bf16[128,2048]{1,0:T(8,128)(2,1)S(1)}, u32[]{:S(2)}, u32[]{:S(2)}) collective-permute-start(bf16[128,2048]{1,0:T(8,128)(2,1)S(1)} %bitcast.31), channel_id=1, source_target_pairs={{0,1},{1,0},{2,3},{3,2},{4,5},{5,4},{6,7},{7,6},{8,9},{9,8},{10,11... | collective-permute-start | bytes 1572872 | tf_op jit(solution)/shard_map/ppermute | solution.py:32
  235.1 2.6 %shard_map.175 = (bf16[128,2048]{1,0:T(8,128)(2,1)S(1)}, bf16[128,2048]{1,0:T(8,128)(2,1)S(1)}) custom-call(bf16[128,2048]{1,0:T(8,128)(2,1)S(1)} %bitcast.32, bf16[128,2048]{1,0:T(8,128)(2,1)S(1)} %collective-permute-done.11.far_ref, bf16[2048,1792]{1,0:T(8,128)(2,1)S(1)} %bitcast.28, bf16[2048,768]{1,0:T(8,128)(2,1)S(1)} %bitcast.30, ...), custom_call_target="tpu_custom_call" | custom-call | flops 2415919104 | bytes 11534336 | tf_op jit(solution)/shard_map/pallas_call | solution.py:157
  237.7 2.3 collective-permute-start.12
  241.6 11.6 %all_to_all.33 = bf16[4,32,2048]{2,1,0:T(8,128)(2,1)S(1)} all-to-all(bf16[4,32,2048]{2,1,0:T(8,128)(2,1)S(1)} %bitcast.36), channel_id=1, replica_groups=mesh['z'=16,'y'=4,'x'=4,'c'=2] {'x'}, dimensions={0} | all-to-all | bytes 1048576 | tf_op jit(solution)/shard_map/all_to_all | solution.py:122
  (90 shorter events, 21.4 us)
Async XLA Ops:
  6.5 94.7 %copy-start.12 = (f32[768]{0:T(1024)S(1)}, f32[768]{0:T(1024)}, u32[]{:S(2)}) copy-start(f32[768]{0:T(1024)} %param.23) | copy-start | bytes 9220
  6.5 94.8 %copy-start.13 = (f32[768]{0:T(1024)S(1)}, f32[768]{0:T(1024)}, u32[]{:S(2)}) copy-start(f32[768]{0:T(1024)} %param.25) | copy-start | bytes 9220
  6.5 94.9 %copy-start.16 = (f32[256]{0:T(256)S(1)}, f32[256]{0:T(256)}, u32[]{:S(2)}) copy-start(f32[256]{0:T(256)} %param.29) | copy-start | bytes 3076
  6.5 94.9 %copy-start.15 = (f32[256]{0:T(256)S(1)}, f32[256]{0:T(256)}, u32[]{:S(2)}) copy-start(f32[256]{0:T(256)} %param.31) | copy-start | bytes 3076
  6.5 94.9 %copy-start.14 = (f32[256]{0:T(256)S(1)}, f32[256]{0:T(256)}, u32[]{:S(2)}) copy-start(f32[256]{0:T(256)} %param.33) | copy-start | bytes 3076
  6.5 121.1 %all-gather.2.cloned.1.call-start = ((), (), s32[]{:S(2)}) async-start(), calls=%async_computation.6 | async-start | bytes 7798784 | tf_op jit(solution)/shard_map/all_gather | solution.py:316
  59.9 41.5 %copy-start.3 = (bf16[512,768]{1,0:T(8,128)(2,1)}, bf16[512,768]{1,0:T(8,128)(2,1)S(1)}, u32[]{:S(2)}) copy-start(bf16[512,768]{1,0:T(8,128)(2,1)S(1)} %all_gather.10) | copy-start | bytes 2359300
  59.9 33.0 %collective-permute-start.1 = (bf16[512,768]{1,0:T(8,128)(2,1)S(1)}, bf16[512,768]{1,0:T(8,128)(2,1)S(1)}, u32[]{:S(2)}, u32[]{:S(2)}) collective-permute-start(bf16[512,768]{1,0:T(8,128)(2,1)S(1)} %all_gather.10), channel_id=1, source_target_pairs={{0,8},{8,16},{16,24},{24,0},{1,9},{9,17},{17,25},{25,1},{2,10},{10... | collective-permute-start | bytes 2359304 | tf_op jit(solution)/shard_map/ppermute | solution.py:37
  61.8 33.6 %collective-permute-start.3 = (bf16[512,768]{1,0:T(8,128)(2,1)S(1)}, bf16[512,768]{1,0:T(8,128)(2,1)S(1)}, u32[]{:S(2)}, u32[]{:S(2)}) collective-permute-start(bf16[512,768]{1,0:T(8,128)(2,1)S(1)} %all_gather.10), channel_id=1, source_target_pairs={{0,24},{8,0},{16,8},{24,16},{1,25},{9,1},{17,9},{25,17},{2,26},{10... | collective-permute-start | bytes 2359304 | tf_op jit(solution)/shard_map/ppermute | solution.py:37
  81.0 22.1 %collective-permute-start = (bf16[128,2048]{1,0:T(8,128)(2,1)}, bf16[128,2048]{1,0:T(8,128)(2,1)}, u32[]{:S(2)}, u32[]{:S(2)}) collective-permute-start(bf16[128,2048]{1,0:T(8,128)(2,1)} %bitcast.4.near_ref), channel_id=1, source_target_pairs={{0,1},{1,0},{2,3},{3,2},{4,5},{5,4},{6,7},{7,6},{8,9},{9,8},{10,11... | collective-permute-start | bytes 1572872 | tf_op jit(solution)/shard_map/ppermute | solution.py:32
  92.9 8.5 %copy-start.7 = (bf16[512,768]{1,0:T(8,128)(2,1)}, bf16[512,768]{1,0:T(8,128)(2,1)S(1)}, u32[]{:S(2)}) copy-start(bf16[512,768]{1,0:T(8,128)(2,1)S(1)} %collective-permute-done.1) | copy-start | bytes 2359300
  93.0 13.9 %collective-permute-start.2 = (bf16[256,768]{1,0:T(8,128)(2,1)S(1)}, bf16[256,768]{1,0:T(8,128)(2,1)}, u32[]{:S(2)}, u32[]{:S(2)}) collective-permute-start(bf16[256,768]{1,0:T(8,128)(2,1)S(1)} %slice.12), channel_id=1, source_target_pairs={{0,8},{8,16},{16,24},{24,0},{1,9},{9,17},{17,25},{25,1},{2,10},{10... | collective-permute-start | bytes 1179656 | tf_op jit(solution)/shard_map/ppermute | solution.py:37
  97.2 12.6 %collective-permute-start.4 = (bf16[256,768]{1,0:T(8,128)(2,1)}, bf16[256,768]{1,0:T(8,128)(2,1)}, u32[]{:S(2)}, u32[]{:S(2)}) collective-permute-start(bf16[256,768]{1,0:T(8,128)(2,1)} %slice.13), channel_id=1, source_target_pairs={{0,24},{8,0},{16,8},{24,16},{1,25},{9,1},{17,9},{25,17},{2,26},{10... | collective-permute-start | bytes 1179656 | tf_op jit(solution)/shard_map/ppermute | solution.py:37
  103.1 8.0 %copy-start.6 = (bf16[512,768]{1,0:T(8,128)(2,1)S(1)}, bf16[512,768]{1,0:T(8,128)(2,1)}, u32[]{:S(2)}) copy-start(bf16[512,768]{1,0:T(8,128)(2,1)} %copy-done.5) | copy-start | bytes 2359300
  111.1 23.4 %copy-start.1 = (bf16[1,16,4,32,768]{4,3,2,1,0:T(8,128)(2,1)}, bf16[1,16,4,32,768]{4,3,2,1,0:T(8,128)(2,1)S(1)}, u32[]{:S(2)}) copy-start(bf16[1,16,4,32,768]{4,3,2,1,0:T(8,128)(2,1)S(1)} %constant_dynamic-update-slice_fusion) | copy-start | bytes 9437188
  127.7 3.1 %copy-start = (bf16[2048,1792]{1,0:T(8,128)(2,1)S(1)}, bf16[2048,1792]{1,0:T(8,128)(2,1)}, u32[]{:S(2)}) copy-start(bf16[2048,1792]{1,0:T(8,128)(2,1)} %all-gather.2.cloned.1.call-done.gate_up) | copy-start | bytes 22020100
  134.6 21.1 %copy-start.9 = (bf16[32,2048]{1,0:T(8,128)(2,1)S(1)}, bf16[32,2048]{1,0:T(8,128)(2,1)}, u32[]{:S(2)}) copy-start(bf16[32,2048]{1,0:T(8,128)(2,1)} %param.18) | copy-start | bytes 393220
  134.6 34.0 %copy-start.10 = (f32[2048]{0:T(1024)S(1)}, f32[2048]{0:T(1024)}, u32[]{:S(2)}) copy-start(f32[2048]{0:T(1024)} %param.20) | copy-start | bytes 24580
  134.6 7.0 %collective-permute-start.5 = (bf16[128,2048]{1,0:T(8,128)(2,1)S(1)}, bf16[128,2048]{1,0:T(8,128)(2,1)S(1)}, u32[]{:S(2)}, u32[]{:S(2)}) collective-permute-start(bf16[128,2048]{1,0:T(8,128)(2,1)S(1)} %get-tuple-element.28), channel_id=1, source_target_pairs={{0,1},{1,0},{2,3},{3,2},{4,5},{5,4},{6,7},{7,6},{8,9},{9,8},{10,11... | collective-permute-start | bytes 1572872 | tf_op jit(solution)/shard_map/ppermute | solution.py:32
  138.5 28.1 %collective-permute-start.7 = (bf16[2048,256]{1,0:T(8,128)(2,1)}, bf16[2048,256]{1,0:T(8,128)(2,1)}, u32[]{:S(2)}, u32[]{:S(2)}) collective-permute-start(bf16[2048,256]{1,0:T(8,128)(2,1)} %slice.14), channel_id=1, source_target_pairs={{0,8},{8,16},{16,24},{24,0},{1,9},{9,17},{17,25},{25,1},{2,10},{10... | collective-permute-start | bytes 3145736 | tf_op jit(solution)/shard_map/ppermute | solution.py:37
  142.6 13.0 %all-to-all-start.1 = ((bf16[4,32,2048]{2,1,0:T(8,128)(2,1)}), bf16[4,32,2048]{2,1,0:T(8,128)(2,1)S(1)}, u32[]{:S(2)}, u32[]{:S(2)}) async-start(bf16[4,32,2048]{2,1,0:T(8,128)(2,1)} %bitcast.15), calls=%async_computation.1 | async-start | bytes 1048576 | tf_op jit(solution)/shard_map/all_to_all | solution.py:122
  146.5 40.2 %collective-permute-start.8 = (bf16[2048,256]{1,0:T(8,128)(2,1)}, bf16[2048,256]{1,0:T(8,128)(2,1)}, u32[]{:S(2)}, u32[]{:S(2)}) collective-permute-start(bf16[2048,256]{1,0:T(8,128)(2,1)} %slice.14), channel_id=1, source_target_pairs={{0,24},{8,0},{16,8},{24,16},{1,25},{9,1},{17,9},{25,17},{2,26},{10... | collective-permute-start | bytes 3145736 | tf_op jit(solution)/shard_map/ppermute | solution.py:37
  166.6 27.3 %collective-permute-start.9 = (bf16[2048,256]{1,0:T(8,128)(2,1)}, bf16[2048,256]{1,0:T(8,128)(2,1)}, u32[]{:S(2)}, u32[]{:S(2)}) collective-permute-start(bf16[2048,256]{1,0:T(8,128)(2,1)} %collective-permute-done.7), channel_id=1, source_target_pairs={{0,8},{8,16},{16,24},{24,0},{1,9},{9,17},{17,25},{25,1},{2,10},{10... | collective-permute-start | bytes 3145736 | tf_op jit(solution)/shard_map/ppermute | solution.py:37
  168.7 66.4 %slice-start = ((s8[7340032]{0:T(1024)(128)(4,1)}), s8[3145728]{0:T(1024)(128)(4,1)S(1)}, s32[]{:S(2)}) async-start(s8[7340032]{0:T(1024)(128)(4,1)} %bitcast.27), calls=%async_computation.7 | async-start | bytes 6291456
  169.5 12.3 %all-to-all-start.2 = ((bf16[4,32,2048]{2,1,0:T(8,128)(2,1)}), bf16[4,32,2048]{2,1,0:T(8,128)(2,1)}, u32[]{:S(2)}, u32[]{:S(2)}) async-start(bf16[4,32,2048]{2,1,0:T(8,128)(2,1)} %broadcast_in_dim.35), calls=%async_computation.2 | async-start | bytes 1048576 | tf_op jit(solution)/shard_map/all_to_all | solution.py:28
  181.9 6.1 %collective-permute-start.6 = (bf16[128,2048]{1,0:T(8,128)(2,1)}, bf16[128,2048]{1,0:T(8,128)(2,1)S(1)}, u32[]{:S(2)}, u32[]{:S(2)}) collective-permute-start(bf16[128,2048]{1,0:T(8,128)(2,1)} %bitcast.16.near_ref), channel_id=1, source_target_pairs={{0,1},{1,0},{2,3},{3,2},{4,5},{5,4},{6,7},{7,6},{8,9},{9,8},{10,11... | collective-permute-start | bytes 1572872 | tf_op jit(solution)/shard_map/ppermute | solution.py:32
  194.0 41.0 %slice-start.1 = ((s8[7340032]{0:T(1024)(128)(4,1)}), s8[4194304]{0:T(1024)(128)(4,1)S(1)}, s32[]{:S(2)}) async-start(s8[7340032]{0:T(1024)(128)(4,1)} %bitcast.27), calls=%async_computation.8 | async-start | bytes 8388608
  200.4 18.2 %copy-start.11 = (f32[2048]{0:T(1024)S(1)}, f32[2048]{0:T(1024)}, u32[]{:S(2)}) copy-start(f32[2048]{0:T(1024)} %param.21) | copy-start | bytes 24580
  200.4 34.6 %copy-start.2 = (bf16[1,16,4,32,768]{4,3,2,1,0:T(8,128)(2,1)S(1)}, bf16[1,16,4,32,768]{4,3,2,1,0:T(8,128)(2,1)}, u32[]{:S(2)}) copy-start(bf16[1,16,4,32,768]{4,3,2,1,0:T(8,128)(2,1)} %copy-done.1) | copy-start | bytes 9437188
  200.4 5.4 %collective-permute-start.10 = (bf16[128,2048]{1,0:T(8,128)(2,1)S(1)}, bf16[128,2048]{1,0:T(8,128)(2,1)S(1)}, u32[]{:S(2)}, u32[]{:S(2)}) collective-permute-start(bf16[128,2048]{1,0:T(8,128)(2,1)S(1)} %get-tuple-element.32), channel_id=1, source_target_pairs={{0,1},{1,0},{2,3},{3,2},{4,5},{5,4},{6,7},{7,6},{8,9},{9,8},{10,11... | collective-permute-start | bytes 1572872 | tf_op jit(solution)/shard_map/ppermute | solution.py:32
  229.0 6.1 %collective-permute-start.11 = (bf16[128,2048]{1,0:T(8,128)(2,1)S(1)}, bf16[128,2048]{1,0:T(8,128)(2,1)S(1)}, u32[]{:S(2)}, u32[]{:S(2)}) collective-permute-start(bf16[128,2048]{1,0:T(8,128)(2,1)S(1)} %bitcast.31), channel_id=1, source_target_pairs={{0,1},{1,0},{2,3},{3,2},{4,5},{5,4},{6,7},{7,6},{8,9},{9,8},{10,11... | collective-permute-start | bytes 1572872 | tf_op jit(solution)/shard_map/ppermute | solution.py:32
  237.7 3.8 %collective-permute-start.12 = (bf16[128,2048]{1,0:T(8,128)(2,1)S(1)}, bf16[128,2048]{1,0:T(8,128)(2,1)S(1)}, u32[]{:S(2)}, u32[]{:S(2)}) collective-permute-start(bf16[128,2048]{1,0:T(8,128)(2,1)S(1)} %get-tuple-element.34), channel_id=1, source_target_pairs={{0,1},{1,0},{2,3},{3,2},{4,5},{5,4},{6,7},{7,6},{8,9},{9,8},{10,11... | collective-permute-start | bytes 1572872 | tf_op jit(solution)/shard_map/ppermute | solution.py:32
  (3 other events, 3.3 us)
Sparse Core Ops, SparseCore 0:
  21.5 106.1 all-gather.1
where the time goes:
time: 262 us; the launch traced here: 261 us
  blocking collectives  96.5 us (37%)
  starting transfers between devices  59.6 us (23%)
  waiting for transfers between devices  59 us (23%)
  Pallas kernels  14.6 us (6%)
  between operations  14.1 us (5%)
  local copies, waits for them, and re-layouts  10.5 us (4%)
  other arithmetic  6.52 us (2%)
    all_gather x1, blocking collectives, layer(): lax.all_gather(after(second_part, packed_y), 'z', axis=0, tiled=True)  38.5 us
    ppermute x6, starting transfers between devices, swapped(): return lax.ppermute(x, 'c', [(0, 1), (1, 0)])  30 us
    all_to_all x2, blocking collectives, return_rows(): arrived = lax.all_to_all(pieces, 'x', 0, 0, tiled=True)  24 us
    ppermute x7, waiting for transfers between devices, shifted(): return lax.ppermute(x, axis, [(i, (i + by) % peers) for i in range(peers)])  23.4 us
    all_to_all x2, blocking collectives, spread(): lax.all_to_all(sent, 'x', 0, 0, tiled=True).reshape(-1, own_rows.shape[1])  22.7 us
    ppermute x7, starting transfers between devices, shifted(): return lax.ppermute(x, axis, [(i, (i + by) % peers) for i in range(peers)])  21.3 us
    all_gather x1, waiting for transfers between devices, layer(): whole_z = lax.all_gather(packed_y, 'z', axis=0, tiled=True)  16.5 us
    all_gather x1, blocking collectives, layer(): packed_y = lax.all_gather(packed, 'y', axis=0, tiled=True)  11.3 us
  transfers between devices with their start and end apart: 16, of which 11 were waited for; matrix products, arithmetic and copies ran while one was open for 4% of the time, Pallas kernels for 0%

commit v1 on v0

--- a/solution.py
+++ b/solution.py
@@ -11,6 +11,7 @@
 HEAD_DIM = 256
 BLOCK = 64
 TOK = 256
+MOVED = 128
 FS = ("z", "y")
 TP = ("x", "c")
 FS_TP = ("z", "y", "x", "c")
@@ -65,12 +66,14 @@
     first_ref, second_ref, third_ref,
 ):
     low = jnp.bfloat16
-    rows, hidden_width = gate_ref.shape
+    rows, units = gate_ref.shape
     width = query_ref.shape[1]
-    first_ref[:, :hidden_width] = gate_ref[...].astype(low)
-    first_ref[:, hidden_width : 2 * hidden_width] = up_ref[...].astype(low)
-    first_ref[:, 2 * hidden_width :] = jnp.zeros((rows, width), low)
-    second_ref[...] = scaled_rows(down_ref[...], down_scale_ref[...])
+    kept = units - MOVED
+    first_ref[:, :units] = gate_ref[...].astype(low)
+    first_ref[:, units : units + kept] = up_ref[:, :kept].astype(low)
+    first_ref[:, units + kept :] = jnp.zeros((rows, width), low)
+    second_ref[:, :units] = scaled_rows(down_ref[...], down_scale_ref[...])
+    second_ref[:, units:] = up_ref[:, kept:].astype(low)
     for k, ref in enumerate((query_ref, key_ref, value_ref)):
         third_ref[pl.ds(k * rows, rows), :] = ref[...].astype(low)
     third_ref[pl.ds(3 * rows, rows), :] = scaled_rows(output_ref[...], output_scale_ref[...])
@@ -85,7 +88,8 @@
 def prepare(gate, up, down, down_scale, query, key, value, output, output_scale):
     rows, hidden_width = gate.shape
     width = query.shape[1]
-    shapes = ((rows, 2 * hidden_width + width), (rows, hidden_width), (4 * rows, width))
+    units = hidden_width
+    shapes = ((rows, 2 * units - MOVED + width), (rows, units + MOVED), (4 * rows, width))
     return pl.pallas_call(
         prepare_kernel,
         out_shape=[jax.ShapeDtypeStruct(x, jnp.bfloat16) for x in shapes],
@@ -134,19 +138,28 @@
 
 def mlp_kernel(near_ref, far_ref, gate_up, down, gate_scale, up_scale, out_near, out_far):
     half, width = near_ref.shape
-    units, tile = down.shape[1], 256
+    units, tile = down.shape[1] - MOVED, 256
+    kept = units - MOVED
     x = jnp.concatenate([near_ref[...], far_ref[...]], axis=0)
     hidden = []
     for first in range(0, units, tile):
         here, there = pl.ds(first, tile), pl.ds(units + first, tile)
         gate = jnp.dot(x, gate_up[:, here], preferred_element_type=jnp.float32)
-        up = jnp.dot(x, gate_up[:, there], preferred_element_type=jnp.float32)
+        if first + tile <= kept:
+            up = jnp.dot(x, gate_up[:, there], preferred_element_type=jnp.float32)
+        else:
+            there = pl.ds(units + first, kept - first)
+            up = [
+                jnp.dot(x, w, preferred_element_type=jnp.float32)
+                for w in (gate_up[:, there], down[:, units:])
+            ]
+            up = jnp.concatenate(up, axis=1)
         gate, up = gate * gate_scale[:, here], up * up_scale[:, here]
         hidden.append((gate / (1.0 + jnp.exp(-gate)) * up).astype(jnp.bfloat16))
     hidden = jnp.concatenate(hidden, axis=1)
     for first in range(0, width, 512):
         here = pl.ds(first, 512)
-        term = product(hidden, down[here, :]).astype(jnp.bfloat16)
+        term = product(hidden, down[here, :units]).astype(jnp.bfloat16)
         out_near[:, here] = term[:half, :]
         out_far[:, here] = term[half:, :]
 
@@ -307,12 +320,13 @@
     low = jnp.bfloat16
     z, rows = lax.axis_size("z"), gate_weight.shape[0]
     hidden_width, local_width = down_weight.shape[0], query_weight.shape[1]
+    first_width = 2 * hidden_width - MOVED
     packed, second_part, third_part = prepare(
         gate_weight, up_weight, down_weight, down_scale, query_weight, key_weight, value_weight,
         output_weight, output_scale,
     )
     packed_y = lax.all_gather(packed, "y", axis=0, tiled=True)
-    packed_y = lax.dynamic_update_slice(packed_y, third_part, (0, 2 * hidden_width))
+    packed_y = lax.dynamic_update_slice(packed_y, third_part, (0, first_width))
     whole_z = lax.all_gather(packed_y, "z", axis=0, tiled=True)
     second_z = lax.all_gather(after(second_part, packed_y), "z", axis=0, tiled=True)
     second_near = y_neighbours(second_z)
@@ -320,11 +334,11 @@
     second_far = y_opposite(*second_near)
     down_full = joined_over_y(
         *[
-            x.reshape(1, z, rows, hidden_width)
+            x.reshape(1, z, rows, hidden_width + MOVED)
             for x in (second_z, *second_near, jnp.concatenate(second_far, axis=0))
         ]
     )[0]
-    third_z = whole_z[:, 2 * hidden_width :]
+    third_z = whole_z[:, first_width:]
     third_below = shifted(third_z, "y", 1)
     third_above = shifted(third_z, "y", -1)
     third_far = shifted(third_below, "y", 1)

time: 262 us -> 259 us (0.989)
  waiting for transfers between devices: 59 us -> 51.9 us
  local copies, waits for them, and re-layouts: 10.5 us -> 13.9 us
    all_gather x1, waiting for transfers between devices: 16.5 us -> 7.21 us  [layer(): whole_z = lax.all_gather(packed_y, 'z', axis=0, tiled=True)]
    unnamed x38 -> x34, local copies, waits for them, and re-layouts: 4.88 us -> 8.44 us
    all_gather x1, blocking collectives: 38.5 us -> 41.3 us  [layer(): lax.all_gather(after(second_part, packed_y), 'z', axis=0, tiled=True)]
    ppermute x7, waiting for transfers between devices: 23.4 us -> 26.2 us  [shifted(): return lax.ppermute(x, axis, [(i, (i + by) % peers) for i in range(peers)])]
where the time goes in v1:
time: 259 us; the launch traced here: 258 us
  blocking collectives  98 us (38%)
  starting transfers between devices  59.4 us (23%)
  waiting for transfers between devices  51.9 us (20%)
  between operations  14 us (5%)
  local copies, waits for them, and re-layouts  13.9 us (5%)
  Pallas kernels  13.8 us (5%)
  other arithmetic  6.6 us (3%)
    all_gather x1, blocking collectives, layer(): lax.all_gather(after(second_part, packed_y), 'z', axis=0, tiled=True)  41.3 us
    ppermute x6, starting transfers between devices, swapped(): return lax.ppermute(x, 'c', [(0, 1), (1, 0)])  29.8 us
    ppermute x7, waiting for transfers between devices, shifted(): return lax.ppermute(x, axis, [(i, (i + by) % peers) for i in range(peers)])  26.2 us
    all_to_all x2, blocking collectives, return_rows(): arrived = lax.all_to_all(pieces, 'x', 0, 0, tiled=True)  24 us
    all_to_all x2, blocking collectives, spread(): lax.all_to_all(sent, 'x', 0, 0, tiled=True).reshape(-1, own_rows.shape[1])  21.4 us
    ppermute x7, starting transfers between devices, shifted(): return lax.ppermute(x, axis, [(i, (i + by) % peers) for i in range(peers)])  21.4 us
    all_gather x1, blocking collectives, layer(): packed_y = lax.all_gather(packed, 'y', axis=0, tiled=True)  11.2 us
    unnamed x34, local copies, waits for them, and re-layouts  8.44 us
  transfers between devices with their start and end apart: 16, of which 11 were waited for; matrix products, arithmetic and copies ran while one was open for 4% of the time, Pallas kernels for 0%

profile of v1, /device:TPU:1, one launch (start us, length us, event | category | flops | bytes accessed | tf_op | source)
XLA Modules:
  0.0 257.6 jit_solution(18186897157440277967)
XLA Ops:
  8.4 11.2 %all_gather.9 = bf16[128,1664]{1,0:T(8,128)(2,1)S(1)} all-gather(bf16[32,1664]{1,0:T(8,128)(2,1)} %get-tuple-element.21), channel_id=1, replica_groups=mesh['z'=16,'y'=4,'x'=4,'c'=2] {'y'}, dimensions={0}, use_global_device_ids=true | all-gather | bytes 532480 | tf_op jit(solution)/shard_map/all_gather | solution.py:328
  21.3 41.3 %all_gather.10 = bf16[512,896]{1,0:T(8,128)(2,1)S(1)} all-gather(bf16[32,896]{1,0:T(8,128)(2,1)} %get-tuple-element.23), channel_id=1, replica_groups=mesh['z'=16,'y'=4,'x'=4,'c'=2] {'z'}, dimensions={0}, use_global_device_ids=true | all-gather | bytes 974848 | tf_op jit(solution)/shard_map/all_gather | solution.py:331
  64.6 4.6 %collective-permute-start.3 = (bf16[512,896]{1,0:T(8,128)(2,1)S(1)}, bf16[512,896]{1,0:T(8,128)(2,1)S(1)}, u32[]{:S(2)}, u32[]{:S(2)}) collective-permute-start(bf16[512,896]{1,0:T(8,128)(2,1)S(1)} %all_gather.10), channel_id=1, source_target_pairs={{0,24},{8,0},{16,8},{24,16},{1,25},{9,1},{17,9},{25,17},{2,26},{10... | collective-permute-start | bytes 2752520 | tf_op jit(solution)/shard_map/ppermute | solution.py:38
  71.3 11.2 %all_to_all.30 = bf16[4,32,2048]{2,1,0:T(8,128)(2,1)S(1)} all-to-all(bf16[4,32,2048]{2,1,0:T(8,128)(2,1)S(1)} %broadcast_in_dim.30), channel_id=1, replica_groups=mesh['z'=16,'y'=4,'x'=4,'c'=2] {'x'}, dimensions={0} | all-to-all | bytes 1048576 | tf_op jit(solution)/shard_map/all_to_all | solution.py:29
  82.5 12.0 %collective-permute-start = (bf16[128,2048]{1,0:T(8,128)(2,1)S(1)}, bf16[128,2048]{1,0:T(8,128)(2,1)S(1)}, u32[]{:S(2)}, u32[]{:S(2)}) collective-permute-start(bf16[128,2048]{1,0:T(8,128)(2,1)S(1)} %bitcast.31), channel_id=1, source_target_pairs={{0,1},{1,0},{2,3},{3,2},{4,5},{5,4},{6,7},{7,6},{8,9},{9,8},{10,11... | collective-permute-start | bytes 1572872 | tf_op jit(solution)/shard_map/ppermute | solution.py:33
  95.4 2.6 %collective-permute-start.2 = (bf16[256,896]{1,0:T(8,128)(2,1)}, bf16[256,896]{1,0:T(8,128)(2,1)}, u32[]{:S(2)}, u32[]{:S(2)}) collective-permute-start(bf16[256,896]{1,0:T(8,128)(2,1)} %slice.12), channel_id=1, source_target_pairs={{0,8},{8,16},{16,24},{24,0},{1,9},{9,17},{17,25},{25,1},{2,10},{10... | collective-permute-start | bytes 1376264 | tf_op jit(solution)/shard_map/ppermute | solution.py:38
  98.9 3.8 %collective-permute-start.4 = (bf16[256,896]{1,0:T(8,128)(2,1)}, bf16[256,896]{1,0:T(8,128)(2,1)}, u32[]{:S(2)}, u32[]{:S(2)}) collective-permute-start(bf16[256,896]{1,0:T(8,128)(2,1)} %slice.13), channel_id=1, source_target_pairs={{0,24},{8,0},{16,8},{24,16},{1,25},{9,1},{17,9},{25,17},{2,26},{10... | collective-permute-start | bytes 1376264 | tf_op jit(solution)/shard_map/ppermute | solution.py:38
  104.2 6.7 %collective-permute-done.2 = bf16[256,896]{1,0:T(8,128)(2,1)} collective-permute-done((bf16[256,896]{1,0:T(8,128)(2,1)}, bf16[256,896]{1,0:T(8,128)(2,1)}, u32[]{:S(2)}, u32[]{:S(2)}) %collective-permute-start.2) | collective-permute-done | bytes 458784 | tf_op jit(solution)/shard_map/ppermute | solution.py:38
  110.9 2.0 collective-permute-done.4
  116.3 7.2 %all-gather.2.cloned.1.call-done.gate_up = bf16[2048,1664]{1,0:T(8,128)(2,1)} async-done(((bf16[128,1664]{1,0:T(8,128)(2,1)}), bf16[2048,1664]{1,0:T(8,128)(2,1)}) %all-gather.2.cloned.1.call-update) | async-done | bytes 6815760 | tf_op jit(solution)/shard_map/all_gather | solution.py:330
  123.5 2.0 copy-done.1
  125.6 2.9 %copy-done.3 = bf16[2048,1664]{1,0:T(8,128)(2,1)S(1)} copy-done((bf16[2048,1664]{1,0:T(8,128)(2,1)S(1)}, bf16[2048,1664]{1,0:T(8,128)(2,1)}, u32[]{:S(2)}) %copy-start.3) | copy-done | bytes 6815768
  128.5 2.9 %shard_map.173 = (bf16[128,2048]{1,0:T(8,128)(2,1)S(1)}, bf16[128,2048]{1,0:T(8,128)(2,1)S(1)}) custom-call(bf16[128,2048]{1,0:T(8,128)(2,1)S(1)} %bitcast.32, bf16[128,2048]{1,0:T(8,128)(2,1)S(1)} %collective-permute-done.far_ref, bf16[2048,1664]{1,0:T(8,128)(2,1)S(1)} %copy-done.3, bf16[2048,896]{1,0:T(8,128)(2,1)S(1)} %bitcast.27, ...), custom_call_target="tpu_custom_call" | custom-call | flops 2415919104 | bytes 11534336 | tf_op jit(solution)/shard_map/pallas_call | solution.py:170
  131.4 2.7 %collective-permute-start.5 = (bf16[128,2048]{1,0:T(8,128)(2,1)S(1)}, bf16[128,2048]{1,0:T(8,128)(2,1)S(1)}, u32[]{:S(2)}, u32[]{:S(2)}) collective-permute-start(bf16[128,2048]{1,0:T(8,128)(2,1)S(1)} %get-tuple-element.28), channel_id=1, source_target_pairs={{0,1},{1,0},{2,3},{3,2},{4,5},{5,4},{6,7},{7,6},{8,9},{9,8},{10,11... | collective-permute-start | bytes 1572872 | tf_op jit(solution)/shard_map/ppermute | solution.py:33
  135.1 2.7 %collective-permute-start.7 = (bf16[2048,256]{1,0:T(8,128)(2,1)}, bf16[2048,256]{1,0:T(8,128)(2,1)}, u32[]{:S(2)}, u32[]{:S(2)}) collective-permute-start(bf16[2048,256]{1,0:T(8,128)(2,1)} %slice.14), channel_id=1, source_target_pairs={{0,8},{8,16},{16,24},{24,0},{1,9},{9,17},{17,25},{25,1},{2,10},{10... | collective-permute-start | bytes 3145736 | tf_op jit(solution)/shard_map/ppermute | solution.py:38
  138.8 4.2 %all-to-all-start.1 = ((bf16[4,32,2048]{2,1,0:T(8,128)(2,1)}), bf16[4,32,2048]{2,1,0:T(8,128)(2,1)S(1)}, u32[]{:S(2)}, u32[]{:S(2)}) async-start(bf16[4,32,2048]{2,1,0:T(8,128)(2,1)} %bitcast.15), calls=%async_computation.1 | async-start | bytes 1048576 | tf_op jit(solution)/shard_map/all_to_all | solution.py:126
  143.0 3.8 %collective-permute-start.8 = (bf16[2048,256]{1,0:T(8,128)(2,1)}, bf16[2048,256]{1,0:T(8,128)(2,1)}, u32[]{:S(2)}, u32[]{:S(2)}) collective-permute-start(bf16[2048,256]{1,0:T(8,128)(2,1)} %slice.14), channel_id=1, source_target_pairs={{0,24},{8,0},{16,8},{24,16},{1,25},{9,1},{17,9},{25,17},{2,26},{10... | collective-permute-start | bytes 3145736 | tf_op jit(solution)/shard_map/ppermute | solution.py:38
  146.8 5.2 %all-to-all-done.1 = bf16[4,32,2048]{2,1,0:T(8,128)(2,1)S(1)} async-done(((bf16[4,32,2048]{2,1,0:T(8,128)(2,1)}), bf16[4,32,2048]{2,1,0:T(8,128)(2,1)S(1)}, u32[]{:S(2)}, u32[]{:S(2)}) %all-to-all-start.1) | async-done | bytes 524320 | tf_op jit(solution)/shard_map/all_to_all | solution.py:126
  152.3 11.0 %collective-permute-done.7 = bf16[2048,256]{1,0:T(8,128)(2,1)} collective-permute-done((bf16[2048,256]{1,0:T(8,128)(2,1)}, bf16[2048,256]{1,0:T(8,128)(2,1)}, u32[]{:S(2)}, u32[]{:S(2)}) %collective-permute-start.7) | collective-permute-done | bytes 1048608 | tf_op jit(solution)/shard_map/ppermute | solution.py:38
  163.3 1.9 collective-permute-start.9
  166.1 4.0 %all-to-all-start.2 = ((bf16[4,32,2048]{2,1,0:T(8,128)(2,1)}), bf16[4,32,2048]{2,1,0:T(8,128)(2,1)S(1)}, u32[]{:S(2)}, u32[]{:S(2)}) async-start(bf16[4,32,2048]{2,1,0:T(8,128)(2,1)} %broadcast_in_dim.35), calls=%async_computation.2 | async-start | bytes 1048576 | tf_op jit(solution)/shard_map/all_to_all | solution.py:29
  170.2 8.0 %all-to-all-done.2 = bf16[4,32,2048]{2,1,0:T(8,128)(2,1)S(1)} async-done(((bf16[4,32,2048]{2,1,0:T(8,128)(2,1)}), bf16[4,32,2048]{2,1,0:T(8,128)(2,1)S(1)}, u32[]{:S(2)}, u32[]{:S(2)}) %all-to-all-start.2) | async-done | bytes 524320 | tf_op jit(solution)/shard_map/all_to_all | solution.py:29
  178.3 4.2 %collective-permute-start.6 = (bf16[128,2048]{1,0:T(8,128)(2,1)S(1)}, bf16[128,2048]{1,0:T(8,128)(2,1)S(1)}, u32[]{:S(2)}, u32[]{:S(2)}) collective-permute-start(bf16[128,2048]{1,0:T(8,128)(2,1)S(1)} %bitcast.33), channel_id=1, source_target_pairs={{0,1},{1,0},{2,3},{3,2},{4,5},{5,4},{6,7},{7,6},{8,9},{9,8},{10,11... | collective-permute-start | bytes 1572872 | tf_op jit(solution)/shard_map/ppermute | solution.py:33
  184.0 6.5 %collective-permute-done.9 = bf16[2048,256]{1,0:T(8,128)(2,1)} collective-permute-done((bf16[2048,256]{1,0:T(8,128)(2,1)}, bf16[2048,256]{1,0:T(8,128)(2,1)}, u32[]{:S(2)}, u32[]{:S(2)}) %collective-permute-start.9) | collective-permute-done | bytes 1048608 | tf_op jit(solution)/shard_map/ppermute | solution.py:38
  190.7 6.2 %shard_map.174 = (bf16[128,2048]{1,0:T(8,128)(2,1)S(1)}, bf16[128,2048]{1,0:T(8,128)(2,1)S(1)}) custom-call(s32[2]{0:T(128)S(1)} %pad_add_fusion.place_ref, bf16[128,2048]{1,0:T(8,128)(2,1)S(1)} %bitcast.34, bf16[128,2048]{1,0:T(8,128)(2,1)S(1)} %collective-permute-done.6.far_ref, bf16[16,4,32,256]{3,2,1,0:T(8,128)(2,1)} %bitcast.17.own_ref, ...), custom_call_target="tpu_custom_call" | custom-call | flops 1342177280 | bytes 6291456 | tf_op jit(solution)/shard_map/pallas_call | solution.py:278
  196.9 3.9 %collective-permute-start.10 = (bf16[128,2048]{1,0:T(8,128)(2,1)S(1)}, bf16[128,2048]{1,0:T(8,128)(2,1)S(1)}, u32[]{:S(2)}, u32[]{:S(2)}) collective-permute-start(bf16[128,2048]{1,0:T(8,128)(2,1)S(1)} %get-tuple-element.32), channel_id=1, source_target_pairs={{0,1},{1,0},{2,3},{3,2},{4,5},{5,4},{6,7},{7,6},{8,9},{9,8},{10,11... | collective-permute-start | bytes 1572872 | tf_op jit(solution)/shard_map/ppermute | solution.py:33
  202.4 12.4 %all_to_all.31 = bf16[4,32,2048]{2,1,0:T(8,128)(2,1)S(1)} all-to-all(bf16[4,32,2048]{2,1,0:T(8,128)(2,1)S(1)} %bitcast.39), channel_id=1, replica_groups=mesh['z'=16,'y'=4,'x'=4,'c'=2] {'x'}, dimensions={0} | all-to-all | bytes 1048576 | tf_op jit(solution)/shard_map/all_to_all | solution.py:126
  215.3 10.2 %all_to_all.32 = bf16[4,32,2048]{2,1,0:T(8,128)(2,1)S(1)} all-to-all(bf16[4,32,2048]{2,1,0:T(8,128)(2,1)S(1)} %broadcast_in_dim.40), channel_id=1, replica_groups=mesh['z'=16,'y'=4,'x'=4,'c'=2] {'x'}, dimensions={0} | all-to-all | bytes 1048576 | tf_op jit(solution)/shard_map/all_to_all | solution.py:29
  225.5 4.7 %collective-permute-start.11 = (bf16[128,2048]{1,0:T(8,128)(2,1)S(1)}, bf16[128,2048]{1,0:T(8,128)(2,1)S(1)}, u32[]{:S(2)}, u32[]{:S(2)}) collective-permute-start(bf16[128,2048]{1,0:T(8,128)(2,1)S(1)} %bitcast.35), channel_id=1, source_target_pairs={{0,1},{1,0},{2,3},{3,2},{4,5},{5,4},{6,7},{7,6},{8,9},{9,8},{10,11... | collective-permute-start | bytes 1572872 | tf_op jit(solution)/shard_map/ppermute | solution.py:33
  231.6 2.9 %shard_map.175 = (bf16[128,2048]{1,0:T(8,128)(2,1)S(1)}, bf16[128,2048]{1,0:T(8,128)(2,1)S(1)}) custom-call(bf16[128,2048]{1,0:T(8,128)(2,1)S(1)} %bitcast.36, bf16[128,2048]{1,0:T(8,128)(2,1)S(1)} %collective-permute-done.11.far_ref, bf16[2048,1664]{1,0:T(8,128)(2,1)S(1)} %bitcast.30, bf16[2048,896]{1,0:T(8,128)(2,1)S(1)} %bitcast.28, ...), custom_call_target="tpu_custom_call" | custom-call | flops 2415919104 | bytes 11534336 | tf_op jit(solution)/shard_map/pallas_call | solution.py:170
  234.5 2.3 collective-permute-start.12
  238.4 11.6 %all_to_all.33 = bf16[4,32,2048]{2,1,0:T(8,128)(2,1)S(1)} all-to-all(bf16[4,32,2048]{2,1,0:T(8,128)(2,1)S(1)} %bitcast.40), channel_id=1, replica_groups=mesh['z'=16,'y'=4,'x'=4,'c'=2] {'x'}, dimensions={0} | all-to-all | bytes 1048576 | tf_op jit(solution)/shard_map/all_to_all | solution.py:126
  (86 shorter events, 24.6 us)
Async XLA Ops:
  6.5 96.2 %copy-start.10 = (f32[768]{0:T(1024)S(1)}, f32[768]{0:T(1024)}, u32[]{:S(2)}) copy-start(f32[768]{0:T(1024)} %param.23) | copy-start | bytes 9220
  6.5 96.3 %copy-start.11 = (f32[768]{0:T(1024)S(1)}, f32[768]{0:T(1024)}, u32[]{:S(2)}) copy-start(f32[768]{0:T(1024)} %param.25) | copy-start | bytes 9220
  6.5 96.4 %copy-start.14 = (f32[256]{0:T(256)S(1)}, f32[256]{0:T(256)}, u32[]{:S(2)}) copy-start(f32[256]{0:T(256)} %param.29) | copy-start | bytes 3076
  6.5 96.4 %copy-start.13 = (f32[256]{0:T(256)S(1)}, f32[256]{0:T(256)}, u32[]{:S(2)}) copy-start(f32[256]{0:T(256)} %param.31) | copy-start | bytes 3076
  6.5 96.4 %copy-start.12 = (f32[256]{0:T(256)S(1)}, f32[256]{0:T(256)}, u32[]{:S(2)}) copy-start(f32[256]{0:T(256)} %param.33) | copy-start | bytes 3076
  6.5 117.0 %all-gather.2.cloned.1.call-start = ((), (), s32[]{:S(2)}) async-start(), calls=%async_computation.6 | async-start | bytes 7241728 | tf_op jit(solution)/shard_map/all_gather | solution.py:330
  62.6 31.9 %collective-permute-start.1 = (bf16[512,896]{1,0:T(8,128)(2,1)S(1)}, bf16[512,896]{1,0:T(8,128)(2,1)S(1)}, u32[]{:S(2)}, u32[]{:S(2)}) collective-permute-start(bf16[512,896]{1,0:T(8,128)(2,1)S(1)} %all_gather.10), channel_id=1, source_target_pairs={{0,8},{8,16},{16,24},{24,0},{1,9},{9,17},{17,25},{25,1},{2,10},{10... | collective-permute-start | bytes 2752520 | tf_op jit(solution)/shard_map/ppermute | solution.py:38
  64.6 33.5 %collective-permute-start.3 = (bf16[512,896]{1,0:T(8,128)(2,1)S(1)}, bf16[512,896]{1,0:T(8,128)(2,1)S(1)}, u32[]{:S(2)}, u32[]{:S(2)}) collective-permute-start(bf16[512,896]{1,0:T(8,128)(2,1)S(1)} %all_gather.10), channel_id=1, source_target_pairs={{0,24},{8,0},{16,8},{24,16},{1,25},{9,1},{17,9},{25,17},{2,26},{10... | collective-permute-start | bytes 2752520 | tf_op jit(solution)/shard_map/ppermute | solution.py:38
  82.5 20.4 %collective-permute-start = (bf16[128,2048]{1,0:T(8,128)(2,1)S(1)}, bf16[128,2048]{1,0:T(8,128)(2,1)S(1)}, u32[]{:S(2)}, u32[]{:S(2)}) collective-permute-start(bf16[128,2048]{1,0:T(8,128)(2,1)S(1)} %bitcast.31), channel_id=1, source_target_pairs={{0,1},{1,0},{2,3},{3,2},{4,5},{5,4},{6,7},{7,6},{8,9},{9,8},{10,11... | collective-permute-start | bytes 1572872 | tf_op jit(solution)/shard_map/ppermute | solution.py:33
  94.5 3.6 %copy-start.4 = (bf16[512,896]{1,0:T(8,128)(2,1)}, bf16[512,896]{1,0:T(8,128)(2,1)S(1)}, u32[]{:S(2)}) copy-start(bf16[512,896]{1,0:T(8,128)(2,1)S(1)} %collective-permute-done.1) | copy-start | bytes 2752516
  95.4 15.5 %collective-permute-start.2 = (bf16[256,896]{1,0:T(8,128)(2,1)}, bf16[256,896]{1,0:T(8,128)(2,1)}, u32[]{:S(2)}, u32[]{:S(2)}) collective-permute-start(bf16[256,896]{1,0:T(8,128)(2,1)} %slice.12), channel_id=1, source_target_pairs={{0,8},{8,16},{16,24},{24,0},{1,9},{9,17},{17,25},{25,1},{2,10},{10... | collective-permute-start | bytes 1376264 | tf_op jit(solution)/shard_map/ppermute | solution.py:38
  98.9 14.0 %collective-permute-start.4 = (bf16[256,896]{1,0:T(8,128)(2,1)}, bf16[256,896]{1,0:T(8,128)(2,1)}, u32[]{:S(2)}, u32[]{:S(2)}) collective-permute-start(bf16[256,896]{1,0:T(8,128)(2,1)} %slice.13), channel_id=1, source_target_pairs={{0,24},{8,0},{16,8},{24,16},{1,25},{9,1},{17,9},{25,17},{2,26},{10... | collective-permute-start | bytes 1376264 | tf_op jit(solution)/shard_map/ppermute | solution.py:38
  102.8 1.2 copy-start.5
  114.4 1.9 copy-start
  123.5 2.0 copy-start.1
  125.6 2.9 %copy-start.3 = (bf16[2048,1664]{1,0:T(8,128)(2,1)S(1)}, bf16[2048,1664]{1,0:T(8,128)(2,1)}, u32[]{:S(2)}) copy-start(bf16[2048,1664]{1,0:T(8,128)(2,1)} %all-gather.2.cloned.1.call-done.gate_up) | copy-start | bytes 20447236
  131.4 20.7 %copy-start.7 = (bf16[32,2048]{1,0:T(8,128)(2,1)S(1)}, bf16[32,2048]{1,0:T(8,128)(2,1)}, u32[]{:S(2)}) copy-start(bf16[32,2048]{1,0:T(8,128)(2,1)} %param.18) | copy-start | bytes 393220
  131.4 33.8 %copy-start.8 = (f32[2048]{0:T(1024)S(1)}, f32[2048]{0:T(1024)}, u32[]{:S(2)}) copy-start(f32[2048]{0:T(1024)} %param.20) | copy-start | bytes 24580
  131.4 6.4 %collective-permute-start.5 = (bf16[128,2048]{1,0:T(8,128)(2,1)S(1)}, bf16[128,2048]{1,0:T(8,128)(2,1)S(1)}, u32[]{:S(2)}, u32[]{:S(2)}) collective-permute-start(bf16[128,2048]{1,0:T(8,128)(2,1)S(1)} %get-tuple-element.28), channel_id=1, source_target_pairs={{0,1},{1,0},{2,3},{3,2},{4,5},{5,4},{6,7},{7,6},{8,9},{9,8},{10,11... | collective-permute-start | bytes 1572872 | tf_op jit(solution)/shard_map/ppermute | solution.py:33
  135.1 28.1 %collective-permute-start.7 = (bf16[2048,256]{1,0:T(8,128)(2,1)}, bf16[2048,256]{1,0:T(8,128)(2,1)}, u32[]{:S(2)}, u32[]{:S(2)}) collective-permute-start(bf16[2048,256]{1,0:T(8,128)(2,1)} %slice.14), channel_id=1, source_target_pairs={{0,8},{8,16},{16,24},{24,0},{1,9},{9,17},{17,25},{25,1},{2,10},{10... | collective-permute-start | bytes 3145736 | tf_op jit(solution)/shard_map/ppermute | solution.py:38
  138.8 92.8 %slice-start = ((s8[6815744]{0:T(1024)(128)(4,1)}), s8[2621440]{0:T(1024)(128)(4,1)S(1)}, s32[]{:S(2)}) async-start(s8[6815744]{0:T(1024)(128)(4,1)} %bitcast.29), calls=%async_computation.7 | async-start | bytes 5242880
  138.8 13.2 %all-to-all-start.1 = ((bf16[4,32,2048]{2,1,0:T(8,128)(2,1)}), bf16[4,32,2048]{2,1,0:T(8,128)(2,1)S(1)}, u32[]{:S(2)}, u32[]{:S(2)}) async-start(bf16[4,32,2048]{2,1,0:T(8,128)(2,1)} %bitcast.15), calls=%async_computation.1 | async-start | bytes 1048576 | tf_op jit(solution)/shard_map/all_to_all | solution.py:126
  143.0 40.1 %collective-permute-start.8 = (bf16[2048,256]{1,0:T(8,128)(2,1)}, bf16[2048,256]{1,0:T(8,128)(2,1)}, u32[]{:S(2)}, u32[]{:S(2)}) collective-permute-start(bf16[2048,256]{1,0:T(8,128)(2,1)} %slice.14), channel_id=1, source_target_pairs={{0,24},{8,0},{16,8},{24,16},{1,25},{9,1},{17,9},{25,17},{2,26},{10... | collective-permute-start | bytes 3145736 | tf_op jit(solution)/shard_map/ppermute | solution.py:38
  163.3 27.3 %collective-permute-start.9 = (bf16[2048,256]{1,0:T(8,128)(2,1)}, bf16[2048,256]{1,0:T(8,128)(2,1)}, u32[]{:S(2)}, u32[]{:S(2)}) collective-permute-start(bf16[2048,256]{1,0:T(8,128)(2,1)} %collective-permute-done.7), channel_id=1, source_target_pairs={{0,8},{8,16},{16,24},{24,0},{1,9},{9,17},{17,25},{25,1},{2,10},{10... | collective-permute-start | bytes 3145736 | tf_op jit(solution)/shard_map/ppermute | solution.py:38
  166.1 12.1 %all-to-all-start.2 = ((bf16[4,32,2048]{2,1,0:T(8,128)(2,1)}), bf16[4,32,2048]{2,1,0:T(8,128)(2,1)S(1)}, u32[]{:S(2)}, u32[]{:S(2)}) async-start(bf16[4,32,2048]{2,1,0:T(8,128)(2,1)} %broadcast_in_dim.35), calls=%async_computation.2 | async-start | bytes 1048576 | tf_op jit(solution)/shard_map/all_to_all | solution.py:29
  178.3 5.7 %collective-permute-start.6 = (bf16[128,2048]{1,0:T(8,128)(2,1)S(1)}, bf16[128,2048]{1,0:T(8,128)(2,1)S(1)}, u32[]{:S(2)}, u32[]{:S(2)}) collective-permute-start(bf16[128,2048]{1,0:T(8,128)(2,1)S(1)} %bitcast.33), channel_id=1, source_target_pairs={{0,1},{1,0},{2,3},{3,2},{4,5},{5,4},{6,7},{7,6},{8,9},{9,8},{10,11... | collective-permute-start | bytes 1572872 | tf_op jit(solution)/shard_map/ppermute | solution.py:33
  190.7 24.5 %copy-start.9 = (f32[2048]{0:T(1024)S(1)}, f32[2048]{0:T(1024)}, u32[]{:S(2)}) copy-start(f32[2048]{0:T(1024)} %param.21) | copy-start | bytes 24580
  190.7 40.9 %slice-start.1 = ((s8[6815744]{0:T(1024)(128)(4,1)}), s8[4194304]{0:T(1024)(128)(4,1)S(1)}, s32[]{:S(2)}) async-start(s8[6815744]{0:T(1024)(128)(4,1)} %bitcast.29), calls=%async_computation.8 | async-start | bytes 8388608
  196.9 34.7 %copy-start.2 = (bf16[1,16,4,32,896]{4,3,2,1,0:T(8,128)(2,1)S(1)}, bf16[1,16,4,32,896]{4,3,2,1,0:T(8,128)(2,1)}, u32[]{:S(2)}) copy-start(bf16[1,16,4,32,896]{4,3,2,1,0:T(8,128)(2,1)} %copy-done) | copy-start | bytes 11010052
  196.9 5.4 %collective-permute-start.10 = (bf16[128,2048]{1,0:T(8,128)(2,1)S(1)}, bf16[128,2048]{1,0:T(8,128)(2,1)S(1)}, u32[]{:S(2)}, u32[]{:S(2)}) collective-permute-start(bf16[128,2048]{1,0:T(8,128)(2,1)S(1)} %get-tuple-element.32), channel_id=1, source_target_pairs={{0,1},{1,0},{2,3},{3,2},{4,5},{5,4},{6,7},{7,6},{8,9},{9,8},{10,11... | collective-permute-start | bytes 1572872 | tf_op jit(solution)/shard_map/ppermute | solution.py:33
  225.5 6.1 %collective-permute-start.11 = (bf16[128,2048]{1,0:T(8,128)(2,1)S(1)}, bf16[128,2048]{1,0:T(8,128)(2,1)S(1)}, u32[]{:S(2)}, u32[]{:S(2)}) collective-permute-start(bf16[128,2048]{1,0:T(8,128)(2,1)S(1)} %bitcast.35), channel_id=1, source_target_pairs={{0,1},{1,0},{2,3},{3,2},{4,5},{5,4},{6,7},{7,6},{8,9},{9,8},{10,11... | collective-permute-start | bytes 1572872 | tf_op jit(solution)/shard_map/ppermute | solution.py:33
  234.5 3.8 %collective-permute-start.12 = (bf16[128,2048]{1,0:T(8,128)(2,1)S(1)}, bf16[128,2048]{1,0:T(8,128)(2,1)S(1)}, u32[]{:S(2)}, u32[]{:S(2)}) collective-permute-start(bf16[128,2048]{1,0:T(8,128)(2,1)S(1)} %get-tuple-element.34), channel_id=1, source_target_pairs={{0,1},{1,0},{2,3},{3,2},{4,5},{5,4},{6,7},{7,6},{8,9},{9,8},{10,11... | collective-permute-start | bytes 1572872 | tf_op jit(solution)/shard_map/ppermute | solution.py:33
  (1 other events, 0.8 us)
Sparse Core Ops, SparseCore 0:
  21.4 102.0 all-gather.1

commit v2 on v1

--- a/solution.py
+++ b/solution.py
@@ -69,9 +69,10 @@
     rows, units = gate_ref.shape
     width = query_ref.shape[1]
     kept = units - MOVED
-    first_ref[:, :units] = gate_ref[...].astype(low)
-    first_ref[:, units : units + kept] = up_ref[:, :kept].astype(low)
-    first_ref[:, units + kept :] = jnp.zeros((rows, width), low)
+    for copy in range(first_ref.shape[0]):
+        first_ref[copy, :, :units] = gate_ref[...].astype(low)
+        first_ref[copy, :, units : units + kept] = up_ref[:, :kept].astype(low)
+        first_ref[copy, :, units + kept :] = jnp.zeros((rows, width), low)
     second_ref[:, :units] = scaled_rows(down_ref[...], down_scale_ref[...])
     second_ref[:, units:] = up_ref[:, kept:].astype(low)
     for k, ref in enumerate((query_ref, key_ref, value_ref)):
@@ -89,7 +90,8 @@
     rows, hidden_width = gate.shape
     width = query.shape[1]
     units = hidden_width
-    shapes = ((rows, 2 * units - MOVED + width), (rows, units + MOVED), (4 * rows, width))
+    first = (lax.axis_size("y"), rows, 2 * units - MOVED + width)
+    shapes = (first, (rows, units + MOVED), (4 * rows, width))
     return pl.pallas_call(
         prepare_kernel,
         out_shape=[jax.ShapeDtypeStruct(x, jnp.bfloat16) for x in shapes],
@@ -325,7 +327,7 @@
         gate_weight, up_weight, down_weight, down_scale, query_weight, key_weight, value_weight,
         output_weight, output_scale,
     )
-    packed_y = lax.all_gather(packed, "y", axis=0, tiled=True)
+    packed_y = lax.all_to_all(packed, "y", 0, 0, tiled=True).reshape(-1, packed.shape[2])
     packed_y = lax.dynamic_update_slice(packed_y, third_part, (0, first_width))
     whole_z = lax.all_gather(packed_y, "z", axis=0, tiled=True)
     second_z = lax.all_gather(after(second_part, packed_y), "z", axis=0, tiled=True)

time: 259 us -> 257 us (level)
  waiting for transfers between devices: 51.9 us -> 48.4 us
    all_to_all x0 -> x1, blocking collectives: none -> 11.4 us  [layer(): lax.all_to_all(packed, 'y', 0, 0, tiled=True).reshape(-1, packed.shape[2])]
    all_gather x1 -> x0, blocking collectives: 11.2 us -> none  [layer(): packed_y = lax.all_gather(packed, 'y', axis=0, tiled=True)]
    all_gather x1, waiting for transfers between devices: 7.21 us -> 4.18 us  [layer(): whole_z = lax.all_gather(packed_y, 'z', axis=0, tiled=True)]
where the time goes in v2:
time: 257 us; the launch traced here: 256 us
  blocking collectives  98.6 us (38%)
  starting transfers between devices  60.2 us (23%)
  waiting for transfers between devices  48.4 us (19%)
  between operations  14 us (5%)
  local copies, waits for them, and re-layouts  13.9 us (5%)
  Pallas kernels  13.9 us (5%)
  other arithmetic  6.58 us (3%)
    all_gather x1, blocking collectives, layer(): lax.all_gather(after(second_part, packed_y), 'z', axis=0, tiled=True)  41.8 us
    ppermute x6, starting transfers between devices, swapped(): return lax.ppermute(x, 'c', [(0, 1), (1, 0)])  30.6 us
    ppermute x7, waiting for transfers between devices, shifted(): return lax.ppermute(x, axis, [(i, (i + by) % peers) for i in range(peers)])  25.5 us
    all_to_all x2, blocking collectives, return_rows(): arrived = lax.all_to_all(pieces, 'x', 0, 0, tiled=True)  24 us
    all_to_all x2, blocking collectives, spread(): lax.all_to_all(sent, 'x', 0, 0, tiled=True).reshape(-1, own_rows.shape[1])  21.4 us
    ppermute x7, starting transfers between devices, shifted(): return lax.ppermute(x, axis, [(i, (i + by) % peers) for i in range(peers)])  21.3 us
    all_to_all x1, blocking collectives, layer(): lax.all_to_all(packed, 'y', 0, 0, tiled=True).reshape(-1, packed.shape[2])  11.4 us
    unnamed x34, local copies, waits for them, and re-layouts  8.44 us
  transfers between devices with their start and end apart: 16, of which 11 were waited for; matrix products, arithmetic and copies ran while one was open for 4% of the time, Pallas kernels for 0%

profile of v2, /device:TPU:1, one launch (start us, length us, event | category | flops | bytes accessed | tf_op | source)
XLA Modules:
  0.0 255.6 jit_solution(16836145148894585155)
XLA Ops:
  6.6 1.9 shard_map.172
  8.5 11.4 %all_to_all.35 = bf16[4,32,1664]{2,1,0:T(8,128)(2,1)S(1)} all-to-all(bf16[4,32,1664]{2,1,0:T(8,128)(2,1)} %get-tuple-element.21), channel_id=1, replica_groups=mesh['z'=16,'y'=4,'x'=4,'c'=2] {'y'}, dimensions={0} | all-to-all | bytes 851968 | tf_op jit(solution)/shard_map/all_to_all | solution.py:330
  21.6 41.8 %all_gather.6 = bf16[512,896]{1,0:T(8,128)(2,1)S(1)} all-gather(bf16[32,896]{1,0:T(8,128)(2,1)} %get-tuple-element.23), channel_id=1, replica_groups=mesh['z'=16,'y'=4,'x'=4,'c'=2] {'z'}, dimensions={0}, use_global_device_ids=true | all-gather | bytes 974848 | tf_op jit(solution)/shard_map/all_gather | solution.py:333
  63.4 2.2 collective-permute-start.1
  65.6 4.3 %collective-permute-start.3 = (bf16[512,896]{1,0:T(8,128)(2,1)S(1)}, bf16[512,896]{1,0:T(8,128)(2,1)S(1)}, u32[]{:S(2)}, u32[]{:S(2)}) collective-permute-start(bf16[512,896]{1,0:T(8,128)(2,1)S(1)} %all_gather.6), channel_id=1, source_target_pairs={{0,24},{8,0},{16,8},{24,16},{1,25},{9,1},{17,9},{25,17},{2,26},{10... | collective-permute-start | bytes 2752520 | tf_op jit(solution)/shard_map/ppermute | solution.py:38
  72.0 11.3 %all_to_all.36 = bf16[4,32,2048]{2,1,0:T(8,128)(2,1)S(1)} all-to-all(bf16[4,32,2048]{2,1,0:T(8,128)(2,1)S(1)} %broadcast_in_dim.30), channel_id=1, replica_groups=mesh['z'=16,'y'=4,'x'=4,'c'=2] {'x'}, dimensions={0} | all-to-all | bytes 1048576 | tf_op jit(solution)/shard_map/all_to_all | solution.py:29
  83.2 12.1 %collective-permute-start = (bf16[128,2048]{1,0:T(8,128)(2,1)S(1)}, bf16[128,2048]{1,0:T(8,128)(2,1)S(1)}, u32[]{:S(2)}, u32[]{:S(2)}) collective-permute-start(bf16[128,2048]{1,0:T(8,128)(2,1)S(1)} %bitcast.32), channel_id=1, source_target_pairs={{0,1},{1,0},{2,3},{3,2},{4,5},{5,4},{6,7},{7,6},{8,9},{9,8},{10,11... | collective-permute-start | bytes 1572872 | tf_op jit(solution)/shard_map/ppermute | solution.py:33
  99.0 4.6 %collective-permute-start.4 = (bf16[256,896]{1,0:T(8,128)(2,1)}, bf16[256,896]{1,0:T(8,128)(2,1)}, u32[]{:S(2)}, u32[]{:S(2)}) collective-permute-start(bf16[256,896]{1,0:T(8,128)(2,1)} %slice.13), channel_id=1, source_target_pairs={{0,24},{8,0},{16,8},{24,16},{1,25},{9,1},{17,9},{25,17},{2,26},{10... | collective-permute-start | bytes 1376264 | tf_op jit(solution)/shard_map/ppermute | solution.py:38
  105.0 6.7 %collective-permute-done.2 = bf16[256,896]{1,0:T(8,128)(2,1)} collective-permute-done((bf16[256,896]{1,0:T(8,128)(2,1)}, bf16[256,896]{1,0:T(8,128)(2,1)}, u32[]{:S(2)}, u32[]{:S(2)}) %collective-permute-start.2) | collective-permute-done | bytes 458784 | tf_op jit(solution)/shard_map/ppermute | solution.py:38
  116.9 4.2 %all-gather.2.cloned.1.call-done.gate_up = bf16[2048,1664]{1,0:T(8,128)(2,1)} async-done(((bf16[128,1664]{1,0:T(8,128)(2,1)}), bf16[2048,1664]{1,0:T(8,128)(2,1)}) %all-gather.2.cloned.1.call-update) | async-done | bytes 6815760 | tf_op jit(solution)/shard_map/all_gather | solution.py:332
  121.1 2.0 copy-done.1
  123.1 2.9 %copy-done.3 = bf16[2048,1664]{1,0:T(8,128)(2,1)S(1)} copy-done((bf16[2048,1664]{1,0:T(8,128)(2,1)S(1)}, bf16[2048,1664]{1,0:T(8,128)(2,1)}, u32[]{:S(2)}) %copy-start.3) | copy-done | bytes 6815768
  126.0 2.9 %shard_map.173 = (bf16[128,2048]{1,0:T(8,128)(2,1)S(1)}, bf16[128,2048]{1,0:T(8,128)(2,1)S(1)}) custom-call(bf16[128,2048]{1,0:T(8,128)(2,1)S(1)} %bitcast.33, bf16[128,2048]{1,0:T(8,128)(2,1)S(1)} %collective-permute-done.far_ref, bf16[2048,1664]{1,0:T(8,128)(2,1)S(1)} %copy-done.3, bf16[2048,896]{1,0:T(8,128)(2,1)S(1)} %bitcast.28, ...), custom_call_target="tpu_custom_call" | custom-call | flops 2415919104 | bytes 11534336 | tf_op jit(solution)/shard_map/pallas_call | solution.py:172
  129.0 3.1 %collective-permute-start.5 = (bf16[128,2048]{1,0:T(8,128)(2,1)S(1)}, bf16[128,2048]{1,0:T(8,128)(2,1)S(1)}, u32[]{:S(2)}, u32[]{:S(2)}) collective-permute-start(bf16[128,2048]{1,0:T(8,128)(2,1)S(1)} %get-tuple-element.28), channel_id=1, source_target_pairs={{0,1},{1,0},{2,3},{3,2},{4,5},{5,4},{6,7},{7,6},{8,9},{9,8},{10,11... | collective-permute-start | bytes 1572872 | tf_op jit(solution)/shard_map/ppermute | solution.py:33
  133.1 3.1 %collective-permute-start.7 = (bf16[2048,256]{1,0:T(8,128)(2,1)}, bf16[2048,256]{1,0:T(8,128)(2,1)}, u32[]{:S(2)}, u32[]{:S(2)}) collective-permute-start(bf16[2048,256]{1,0:T(8,128)(2,1)} %slice.14), channel_id=1, source_target_pairs={{0,8},{8,16},{16,24},{24,0},{1,9},{9,17},{17,25},{25,1},{2,10},{10... | collective-permute-start | bytes 3145736 | tf_op jit(solution)/shard_map/ppermute | solution.py:38
  137.2 4.2 %all-to-all-start.2 = ((bf16[4,32,2048]{2,1,0:T(8,128)(2,1)}), bf16[4,32,2048]{2,1,0:T(8,128)(2,1)S(1)}, u32[]{:S(2)}, u32[]{:S(2)}) async-start(bf16[4,32,2048]{2,1,0:T(8,128)(2,1)} %bitcast.16), calls=%async_computation.2 | async-start | bytes 1048576 | tf_op jit(solution)/shard_map/all_to_all | solution.py:128
  141.4 3.4 %collective-permute-start.8 = (bf16[2048,256]{1,0:T(8,128)(2,1)}, bf16[2048,256]{1,0:T(8,128)(2,1)}, u32[]{:S(2)}, u32[]{:S(2)}) collective-permute-start(bf16[2048,256]{1,0:T(8,128)(2,1)} %slice.14), channel_id=1, source_target_pairs={{0,24},{8,0},{16,8},{24,16},{1,25},{9,1},{17,9},{25,17},{2,26},{10... | collective-permute-start | bytes 3145736 | tf_op jit(solution)/shard_map/ppermute | solution.py:38
  144.8 5.6 %all-to-all-done.2 = bf16[4,32,2048]{2,1,0:T(8,128)(2,1)S(1)} async-done(((bf16[4,32,2048]{2,1,0:T(8,128)(2,1)}), bf16[4,32,2048]{2,1,0:T(8,128)(2,1)S(1)}, u32[]{:S(2)}, u32[]{:S(2)}) %all-to-all-start.2) | async-done | bytes 524320 | tf_op jit(solution)/shard_map/all_to_all | solution.py:128
  150.7 10.6 %collective-permute-done.7 = bf16[2048,256]{1,0:T(8,128)(2,1)} collective-permute-done((bf16[2048,256]{1,0:T(8,128)(2,1)}, bf16[2048,256]{1,0:T(8,128)(2,1)}, u32[]{:S(2)}, u32[]{:S(2)}) %collective-permute-start.7) | collective-permute-done | bytes 1048608 | tf_op jit(solution)/shard_map/ppermute | solution.py:38
  161.2 1.9 collective-permute-start.9
  164.1 4.0 %all-to-all-start.3 = ((bf16[4,32,2048]{2,1,0:T(8,128)(2,1)}), bf16[4,32,2048]{2,1,0:T(8,128)(2,1)S(1)}, u32[]{:S(2)}, u32[]{:S(2)}) async-start(bf16[4,32,2048]{2,1,0:T(8,128)(2,1)} %broadcast_in_dim.35), calls=%async_computation.3 | async-start | bytes 1048576 | tf_op jit(solution)/shard_map/all_to_all | solution.py:29
  168.2 7.8 %all-to-all-done.3 = bf16[4,32,2048]{2,1,0:T(8,128)(2,1)S(1)} async-done(((bf16[4,32,2048]{2,1,0:T(8,128)(2,1)}), bf16[4,32,2048]{2,1,0:T(8,128)(2,1)S(1)}, u32[]{:S(2)}, u32[]{:S(2)}) %all-to-all-start.3) | async-done | bytes 524320 | tf_op jit(solution)/shard_map/all_to_all | solution.py:29
  176.0 4.5 %collective-permute-start.6 = (bf16[128,2048]{1,0:T(8,128)(2,1)S(1)}, bf16[128,2048]{1,0:T(8,128)(2,1)S(1)}, u32[]{:S(2)}, u32[]{:S(2)}) collective-permute-start(bf16[128,2048]{1,0:T(8,128)(2,1)S(1)} %bitcast.34), channel_id=1, source_target_pairs={{0,1},{1,0},{2,3},{3,2},{4,5},{5,4},{6,7},{7,6},{8,9},{9,8},{10,11... | collective-permute-start | bytes 1572872 | tf_op jit(solution)/shard_map/ppermute | solution.py:33
  181.9 6.5 %collective-permute-done.9 = bf16[2048,256]{1,0:T(8,128)(2,1)} collective-permute-done((bf16[2048,256]{1,0:T(8,128)(2,1)}, bf16[2048,256]{1,0:T(8,128)(2,1)}, u32[]{:S(2)}, u32[]{:S(2)}) %collective-permute-start.9) | collective-permute-done | bytes 1048608 | tf_op jit(solution)/shard_map/ppermute | solution.py:38
  188.7 6.2 %shard_map.174 = (bf16[128,2048]{1,0:T(8,128)(2,1)S(1)}, bf16[128,2048]{1,0:T(8,128)(2,1)S(1)}) custom-call(s32[2]{0:T(128)S(1)} %pad_add_fusion.place_ref, bf16[128,2048]{1,0:T(8,128)(2,1)S(1)} %bitcast.35, bf16[128,2048]{1,0:T(8,128)(2,1)S(1)} %collective-permute-done.6.far_ref, bf16[16,4,32,256]{3,2,1,0:T(8,128)(2,1)} %bitcast.18.own_ref, ...), custom_call_target="tpu_custom_call" | custom-call | flops 1342177280 | bytes 6291456 | tf_op jit(solution)/shard_map/pallas_call | solution.py:280
  194.9 3.9 %collective-permute-start.10 = (bf16[128,2048]{1,0:T(8,128)(2,1)S(1)}, bf16[128,2048]{1,0:T(8,128)(2,1)S(1)}, u32[]{:S(2)}, u32[]{:S(2)}) collective-permute-start(bf16[128,2048]{1,0:T(8,128)(2,1)S(1)} %get-tuple-element.32), channel_id=1, source_target_pairs={{0,1},{1,0},{2,3},{3,2},{4,5},{5,4},{6,7},{7,6},{8,9},{9,8},{10,11... | collective-permute-start | bytes 1572872 | tf_op jit(solution)/shard_map/ppermute | solution.py:33
  200.4 12.4 %all_to_all.37 = bf16[4,32,2048]{2,1,0:T(8,128)(2,1)S(1)} all-to-all(bf16[4,32,2048]{2,1,0:T(8,128)(2,1)S(1)} %bitcast.40), channel_id=1, replica_groups=mesh['z'=16,'y'=4,'x'=4,'c'=2] {'x'}, dimensions={0} | all-to-all | bytes 1048576 | tf_op jit(solution)/shard_map/all_to_all | solution.py:128
  213.2 10.2 %all_to_all.38 = bf16[4,32,2048]{2,1,0:T(8,128)(2,1)S(1)} all-to-all(bf16[4,32,2048]{2,1,0:T(8,128)(2,1)S(1)} %broadcast_in_dim.40), channel_id=1, replica_groups=mesh['z'=16,'y'=4,'x'=4,'c'=2] {'x'}, dimensions={0} | all-to-all | bytes 1048576 | tf_op jit(solution)/shard_map/all_to_all | solution.py:29
  223.4 4.7 %collective-permute-start.11 = (bf16[128,2048]{1,0:T(8,128)(2,1)S(1)}, bf16[128,2048]{1,0:T(8,128)(2,1)S(1)}, u32[]{:S(2)}, u32[]{:S(2)}) collective-permute-start(bf16[128,2048]{1,0:T(8,128)(2,1)S(1)} %bitcast.36), channel_id=1, source_target_pairs={{0,1},{1,0},{2,3},{3,2},{4,5},{5,4},{6,7},{7,6},{8,9},{9,8},{10,11... | collective-permute-start | bytes 1572872 | tf_op jit(solution)/shard_map/ppermute | solution.py:33
  229.5 2.9 %shard_map.175 = (bf16[128,2048]{1,0:T(8,128)(2,1)S(1)}, bf16[128,2048]{1,0:T(8,128)(2,1)S(1)}) custom-call(bf16[128,2048]{1,0:T(8,128)(2,1)S(1)} %bitcast.37, bf16[128,2048]{1,0:T(8,128)(2,1)S(1)} %collective-permute-done.11.far_ref, bf16[2048,1664]{1,0:T(8,128)(2,1)S(1)} %bitcast.31, bf16[2048,896]{1,0:T(8,128)(2,1)S(1)} %bitcast.29, ...), custom_call_target="tpu_custom_call" | custom-call | flops 2415919104 | bytes 11534336 | tf_op jit(solution)/shard_map/pallas_call | solution.py:172
  232.4 2.3 collective-permute-start.12
  236.3 11.6 %all_to_all.39 = bf16[4,32,2048]{2,1,0:T(8,128)(2,1)S(1)} all-to-all(bf16[4,32,2048]{2,1,0:T(8,128)(2,1)S(1)} %bitcast.41), channel_id=1, replica_groups=mesh['z'=16,'y'=4,'x'=4,'c'=2] {'x'}, dimensions={0} | all-to-all | bytes 1048576 | tf_op jit(solution)/shard_map/all_to_all | solution.py:128
  (86 shorter events, 24.5 us)
Async XLA Ops:
  6.5 97.1 %copy-start.10 = (f32[768]{0:T(1024)S(1)}, f32[768]{0:T(1024)}, u32[]{:S(2)}) copy-start(f32[768]{0:T(1024)} %param.23) | copy-start | bytes 9220
  6.5 97.1 %copy-start.11 = (f32[768]{0:T(1024)S(1)}, f32[768]{0:T(1024)}, u32[]{:S(2)}) copy-start(f32[768]{0:T(1024)} %param.25) | copy-start | bytes 9220
  6.5 97.2 %copy-start.14 = (f32[256]{0:T(256)S(1)}, f32[256]{0:T(256)}, u32[]{:S(2)}) copy-start(f32[256]{0:T(256)} %param.29) | copy-start | bytes 3076
  6.5 97.2 %copy-start.13 = (f32[256]{0:T(256)S(1)}, f32[256]{0:T(256)}, u32[]{:S(2)}) copy-start(f32[256]{0:T(256)} %param.31) | copy-start | bytes 3076
  6.5 97.2 %copy-start.12 = (f32[256]{0:T(256)S(1)}, f32[256]{0:T(256)}, u32[]{:S(2)}) copy-start(f32[256]{0:T(256)} %param.33) | copy-start | bytes 3076
  6.5 114.5 %all-gather.2.cloned.1.call-start = ((), (), s32[]{:S(2)}) async-start(), calls=%async_computation.7 | async-start | bytes 7241728 | tf_op jit(solution)/shard_map/all_gather | solution.py:332
  63.4 32.0 %collective-permute-start.1 = (bf16[512,896]{1,0:T(8,128)(2,1)S(1)}, bf16[512,896]{1,0:T(8,128)(2,1)S(1)}, u32[]{:S(2)}, u32[]{:S(2)}) collective-permute-start(bf16[512,896]{1,0:T(8,128)(2,1)S(1)} %all_gather.6), channel_id=1, source_target_pairs={{0,8},{8,16},{16,24},{24,0},{1,9},{9,17},{17,25},{25,1},{2,10},{10... | collective-permute-start | bytes 2752520 | tf_op jit(solution)/shard_map/ppermute | solution.py:38
  65.6 32.6 %collective-permute-start.3 = (bf16[512,896]{1,0:T(8,128)(2,1)S(1)}, bf16[512,896]{1,0:T(8,128)(2,1)S(1)}, u32[]{:S(2)}, u32[]{:S(2)}) collective-permute-start(bf16[512,896]{1,0:T(8,128)(2,1)S(1)} %all_gather.6), channel_id=1, source_target_pairs={{0,24},{8,0},{16,8},{24,16},{1,25},{9,1},{17,9},{25,17},{2,26},{10... | collective-permute-start | bytes 2752520 | tf_op jit(solution)/shard_map/ppermute | solution.py:38
  83.2 20.5 %collective-permute-start = (bf16[128,2048]{1,0:T(8,128)(2,1)S(1)}, bf16[128,2048]{1,0:T(8,128)(2,1)S(1)}, u32[]{:S(2)}, u32[]{:S(2)}) collective-permute-start(bf16[128,2048]{1,0:T(8,128)(2,1)S(1)} %bitcast.32), channel_id=1, source_target_pairs={{0,1},{1,0},{2,3},{3,2},{4,5},{5,4},{6,7},{7,6},{8,9},{9,8},{10,11... | collective-permute-start | bytes 1572872 | tf_op jit(solution)/shard_map/ppermute | solution.py:33
  95.3 2.8 %copy-start.4 = (bf16[512,896]{1,0:T(8,128)(2,1)}, bf16[512,896]{1,0:T(8,128)(2,1)S(1)}, u32[]{:S(2)}) copy-start(bf16[512,896]{1,0:T(8,128)(2,1)S(1)} %collective-permute-done.1) | copy-start | bytes 2752516
  96.2 15.5 %collective-permute-start.2 = (bf16[256,896]{1,0:T(8,128)(2,1)}, bf16[256,896]{1,0:T(8,128)(2,1)}, u32[]{:S(2)}, u32[]{:S(2)}) collective-permute-start(bf16[256,896]{1,0:T(8,128)(2,1)} %slice.12), channel_id=1, source_target_pairs={{0,8},{8,16},{16,24},{24,0},{1,9},{9,17},{17,25},{25,1},{2,10},{10... | collective-permute-start | bytes 1376264 | tf_op jit(solution)/shard_map/ppermute | solution.py:38
  99.0 14.4 %collective-permute-start.4 = (bf16[256,896]{1,0:T(8,128)(2,1)}, bf16[256,896]{1,0:T(8,128)(2,1)}, u32[]{:S(2)}, u32[]{:S(2)}) collective-permute-start(bf16[256,896]{1,0:T(8,128)(2,1)} %slice.13), channel_id=1, source_target_pairs={{0,24},{8,0},{16,8},{24,16},{1,25},{9,1},{17,9},{25,17},{2,26},{10... | collective-permute-start | bytes 1376264 | tf_op jit(solution)/shard_map/ppermute | solution.py:38
  103.7 1.2 copy-start.5
  115.0 1.9 copy-start
  121.1 2.0 copy-start.1
  123.1 2.9 %copy-start.3 = (bf16[2048,1664]{1,0:T(8,128)(2,1)S(1)}, bf16[2048,1664]{1,0:T(8,128)(2,1)}, u32[]{:S(2)}) copy-start(bf16[2048,1664]{1,0:T(8,128)(2,1)} %all-gather.2.cloned.1.call-done.gate_up) | copy-start | bytes 20447236
  128.9 21.6 %copy-start.7 = (bf16[32,2048]{1,0:T(8,128)(2,1)S(1)}, bf16[32,2048]{1,0:T(8,128)(2,1)}, u32[]{:S(2)}) copy-start(bf16[32,2048]{1,0:T(8,128)(2,1)} %param.18) | copy-start | bytes 393220
  128.9 34.2 %copy-start.8 = (f32[2048]{0:T(1024)S(1)}, f32[2048]{0:T(1024)}, u32[]{:S(2)}) copy-start(f32[2048]{0:T(1024)} %param.20) | copy-start | bytes 24580
  129.0 7.3 %collective-permute-start.5 = (bf16[128,2048]{1,0:T(8,128)(2,1)S(1)}, bf16[128,2048]{1,0:T(8,128)(2,1)S(1)}, u32[]{:S(2)}, u32[]{:S(2)}) collective-permute-start(bf16[128,2048]{1,0:T(8,128)(2,1)S(1)} %get-tuple-element.28), channel_id=1, source_target_pairs={{0,1},{1,0},{2,3},{3,2},{4,5},{5,4},{6,7},{7,6},{8,9},{9,8},{10,11... | collective-permute-start | bytes 1572872 | tf_op jit(solution)/shard_map/ppermute | solution.py:33
  133.1 28.1 %collective-permute-start.7 = (bf16[2048,256]{1,0:T(8,128)(2,1)}, bf16[2048,256]{1,0:T(8,128)(2,1)}, u32[]{:S(2)}, u32[]{:S(2)}) collective-permute-start(bf16[2048,256]{1,0:T(8,128)(2,1)} %slice.14), channel_id=1, source_target_pairs={{0,8},{8,16},{16,24},{24,0},{1,9},{9,17},{17,25},{25,1},{2,10},{10... | collective-permute-start | bytes 3145736 | tf_op jit(solution)/shard_map/ppermute | solution.py:38
  137.2 92.3 %slice-start = ((s8[6815744]{0:T(1024)(128)(4,1)}), s8[2621440]{0:T(1024)(128)(4,1)S(1)}, s32[]{:S(2)}) async-start(s8[6815744]{0:T(1024)(128)(4,1)} %bitcast.30), calls=%async_computation.8 | async-start | bytes 5242880
  137.2 13.2 %all-to-all-start.2 = ((bf16[4,32,2048]{2,1,0:T(8,128)(2,1)}), bf16[4,32,2048]{2,1,0:T(8,128)(2,1)S(1)}, u32[]{:S(2)}, u32[]{:S(2)}) async-start(bf16[4,32,2048]{2,1,0:T(8,128)(2,1)} %bitcast.16), calls=%async_computation.2 | async-start | bytes 1048576 | tf_op jit(solution)/shard_map/all_to_all | solution.py:128
  141.4 39.6 %collective-permute-start.8 = (bf16[2048,256]{1,0:T(8,128)(2,1)}, bf16[2048,256]{1,0:T(8,128)(2,1)}, u32[]{:S(2)}, u32[]{:S(2)}) collective-permute-start(bf16[2048,256]{1,0:T(8,128)(2,1)} %slice.14), channel_id=1, source_target_pairs={{0,24},{8,0},{16,8},{24,16},{1,25},{9,1},{17,9},{25,17},{2,26},{10... | collective-permute-start | bytes 3145736 | tf_op jit(solution)/shard_map/ppermute | solution.py:38
  161.2 27.3 %collective-permute-start.9 = (bf16[2048,256]{1,0:T(8,128)(2,1)}, bf16[2048,256]{1,0:T(8,128)(2,1)}, u32[]{:S(2)}, u32[]{:S(2)}) collective-permute-start(bf16[2048,256]{1,0:T(8,128)(2,1)} %collective-permute-done.7), channel_id=1, source_target_pairs={{0,8},{8,16},{16,24},{24,0},{1,9},{9,17},{17,25},{25,1},{2,10},{10... | collective-permute-start | bytes 3145736 | tf_op jit(solution)/shard_map/ppermute | solution.py:38
  164.1 11.8 %all-to-all-start.3 = ((bf16[4,32,2048]{2,1,0:T(8,128)(2,1)}), bf16[4,32,2048]{2,1,0:T(8,128)(2,1)S(1)}, u32[]{:S(2)}, u32[]{:S(2)}) async-start(bf16[4,32,2048]{2,1,0:T(8,128)(2,1)} %broadcast_in_dim.35), calls=%async_computation.3 | async-start | bytes 1048576 | tf_op jit(solution)/shard_map/all_to_all | solution.py:29
  176.0 6.0 %collective-permute-start.6 = (bf16[128,2048]{1,0:T(8,128)(2,1)S(1)}, bf16[128,2048]{1,0:T(8,128)(2,1)S(1)}, u32[]{:S(2)}, u32[]{:S(2)}) collective-permute-start(bf16[128,2048]{1,0:T(8,128)(2,1)S(1)} %bitcast.34), channel_id=1, source_target_pairs={{0,1},{1,0},{2,3},{3,2},{4,5},{5,4},{6,7},{7,6},{8,9},{9,8},{10,11... | collective-permute-start | bytes 1572872 | tf_op jit(solution)/shard_map/ppermute | solution.py:33
  188.6 24.4 %copy-start.9 = (f32[2048]{0:T(1024)S(1)}, f32[2048]{0:T(1024)}, u32[]{:S(2)}) copy-start(f32[2048]{0:T(1024)} %param.21) | copy-start | bytes 24580
  188.7 40.8 %slice-start.1 = ((s8[6815744]{0:T(1024)(128)(4,1)}), s8[4194304]{0:T(1024)(128)(4,1)S(1)}, s32[]{:S(2)}) async-start(s8[6815744]{0:T(1024)(128)(4,1)} %bitcast.30), calls=%async_computation.9 | async-start | bytes 8388608
  194.9 34.6 %copy-start.2 = (bf16[1,16,4,32,896]{4,3,2,1,0:T(8,128)(2,1)S(1)}, bf16[1,16,4,32,896]{4,3,2,1,0:T(8,128)(2,1)}, u32[]{:S(2)}) copy-start(bf16[1,16,4,32,896]{4,3,2,1,0:T(8,128)(2,1)} %copy-done) | copy-start | bytes 11010052
  194.9 5.4 %collective-permute-start.10 = (bf16[128,2048]{1,0:T(8,128)(2,1)S(1)}, bf16[128,2048]{1,0:T(8,128)(2,1)S(1)}, u32[]{:S(2)}, u32[]{:S(2)}) collective-permute-start(bf16[128,2048]{1,0:T(8,128)(2,1)S(1)} %get-tuple-element.32), channel_id=1, source_target_pairs={{0,1},{1,0},{2,3},{3,2},{4,5},{5,4},{6,7},{7,6},{8,9},{9,8},{10,11... | collective-permute-start | bytes 1572872 | tf_op jit(solution)/shard_map/ppermute | solution.py:33
  223.4 6.1 %collective-permute-start.11 = (bf16[128,2048]{1,0:T(8,128)(2,1)S(1)}, bf16[128,2048]{1,0:T(8,128)(2,1)S(1)}, u32[]{:S(2)}, u32[]{:S(2)}) collective-permute-start(bf16[128,2048]{1,0:T(8,128)(2,1)S(1)} %bitcast.36), channel_id=1, source_target_pairs={{0,1},{1,0},{2,3},{3,2},{4,5},{5,4},{6,7},{7,6},{8,9},{9,8},{10,11... | collective-permute-start | bytes 1572872 | tf_op jit(solution)/shard_map/ppermute | solution.py:33
  232.4 3.8 %collective-permute-start.12 = (bf16[128,2048]{1,0:T(8,128)(2,1)S(1)}, bf16[128,2048]{1,0:T(8,128)(2,1)S(1)}, u32[]{:S(2)}, u32[]{:S(2)}) collective-permute-start(bf16[128,2048]{1,0:T(8,128)(2,1)S(1)} %get-tuple-element.34), channel_id=1, source_target_pairs={{0,1},{1,0},{2,3},{3,2},{4,5},{5,4},{6,7},{7,6},{8,9},{9,8},{10,11... | collective-permute-start | bytes 1572872 | tf_op jit(solution)/shard_map/ppermute | solution.py:33
  (1 other events, 0.8 us)
Sparse Core Ops, SparseCore 0:
  21.7 99.3 all-gather.1

commit v3 on v2

--- a/solution.py
+++ b/solution.py
@@ -136,6 +136,22 @@
 
 VMEM = pl.BlockSpec(memory_space=pltpu.VMEM)
 KERNEL_PARAMS = pltpu.CompilerParams(vmem_limit_bytes=20 * 1024 * 1024)
+
+
+def fetching_mlp_kernel(
+    near_ref, far_ref, gate_up_ref, down_ref, gate_scale, up_scale, out_near, out_far, gate_up, down, arrived
+):
+    depth = gate_up.shape[0] // 4
+    copies = [
+        pltpu.make_async_copy(gate_up_ref.at[here, :], gate_up.at[here, :], arrived.at[k])
+        for k, here in enumerate(pl.ds(k * depth, depth) for k in range(4))
+    ]
+    copies.append(pltpu.make_async_copy(down_ref, down, arrived.at[4]))
+    for copy in copies:
+        copy.start()
+    for copy in copies:
+        copy.wait()
+    mlp_kernel(near_ref, far_ref, gate_up, down, gate_scale, up_scale, out_near, out_far)
 
 
 def mlp_kernel(near_ref, far_ref, gate_up, down, gate_scale, up_scale, out_near, out_far):
@@ -166,15 +182,22 @@
         out_far[:, here] = term[half:, :]
 
 
-def mlp(near, far, gate_up, down_turned, gate_scale, up_scale):
+def mlp(near, far, gate_up, down_turned, gate_scale, up_scale, fetch=False):
     half, width = near.shape
     units = gate_scale.shape[0]
+    weights, scratch, params = [VMEM] * 2, [], KERNEL_PARAMS
+    if fetch:
+        weights = [pl.BlockSpec(memory_space=pl.ANY)] * 2
+        scratch = [pltpu.VMEM(x.shape, jnp.bfloat16) for x in (gate_up, down_turned)]
+        scratch.append(pltpu.SemaphoreType.DMA((5,)))
+        params = pltpu.CompilerParams(vmem_limit_bytes=60 * 1024 * 1024)
     return pl.pallas_call(
-        mlp_kernel,
-        in_specs=[VMEM] * 6,
+        fetching_mlp_kernel if fetch else mlp_kernel,
+        in_specs=[VMEM] * 2 + weights + [VMEM] * 2,
         out_specs=[VMEM] * 2,
         out_shape=[jax.ShapeDtypeStruct((half, width), jnp.bfloat16)] * 2,
-        compiler_params=KERNEL_PARAMS,
+        scratch_shapes=scratch,
+        compiler_params=params,
         cost_estimate=pl.CostEstimate(
             flops=12 * half * width * units,
             bytes_accessed=6 * width * units + 8 * half * width,
@@ -349,7 +372,7 @@
     scales = jnp.concatenate([query_scale, key_scale, value_scale])
     place = jnp.stack([core, lax.axis_index("y")]).astype(jnp.int32)
     first_rows, scales, place = lax.optimization_barrier((first_rows, scales, place))
-    first_term = mlp(*first_rows, whole_z, down_full, gate_scale, up_scale)
+    first_term = mlp(*first_rows, whole_z, down_full, gate_scale, up_scale, fetch=True)
     tables = mixer_tables(TOK, rate)
     mlp_first = return_rows(*first_term)
     pieces = [

time: 257 us -> 261 us (1.016)
  Pallas kernels: 13.9 us -> 22.2 us
  waiting for transfers between devices: 48.4 us -> 44.4 us
    pallas_call x2, Pallas kernels: 5.78 us -> 14.1 us  [mlp(): pl.pallas_call(fetching_mlp_kernel if fetch else mlp_kernel, in_specs=[VM...]
    unnamed x34, local copies, waits for them, and re-layouts: 8.44 us -> 0.85 us
    ppermute x7, waiting for transfers between devices: 25.5 us -> 21.4 us  [shifted(): return lax.ppermute(x, axis, [(i, (i + by) % peers) for i in range(peers)])]
    dynamic_update_slice x3, local copies, waits for them, and re-layouts: 0.46 us -> 3.11 us  [joined_over_y(): whole = lax.dynamic_update_slice(whole, piece[:, :, None], place)]
  transfers between devices with their start and end apart: 16 -> 16, of which waited for: 11 -> 11; matrix products, arithmetic and copies ran while one was open for 4% -> 7% of each run, Pallas kernels for 0% -> 0%
where the time goes in v3:
time: 261 us; the launch traced here: 260 us
  blocking collectives  98.6 us (38%)
  starting transfers between devices  59.9 us (23%)
  waiting for transfers between devices  44.4 us (17%)
  Pallas kernels  22.2 us (9%)
  between operations  13.9 us (5%)
  local copies, waits for them, and re-layouts  13.2 us (5%)
  other arithmetic  7.61 us (3%)
    all_gather x1, blocking collectives, layer(): lax.all_gather(after(second_part, packed_y), 'z', axis=0, tiled=True)  41.8 us
    ppermute x6, starting transfers between devices, swapped(): return lax.ppermute(x, 'c', [(0, 1), (1, 0)])  30.3 us
    all_to_all x2, blocking collectives, return_rows(): arrived = lax.all_to_all(pieces, 'x', 0, 0, tiled=True)  24 us
    all_to_all x2, blocking collectives, spread(): lax.all_to_all(sent, 'x', 0, 0, tiled=True).reshape(-1, own_rows.shape[1])  21.4 us
    ppermute x7, waiting for transfers between devices, shifted(): return lax.ppermute(x, axis, [(i, (i + by) % peers) for i in range(peers)])  21.4 us
    ppermute x7, starting transfers between devices, shifted(): return lax.ppermute(x, axis, [(i, (i + by) % peers) for i in range(peers)])  21.3 us
    pallas_call x2, Pallas kernels, mlp(): pl.pallas_call(fetching_mlp_kernel if fetch else mlp_kernel, in_specs=[VM...  14.1 us
    all_to_all x1, blocking collectives, layer(): lax.all_to_all(packed, 'y', 0, 0, tiled=True).reshape(-1, packed.shape[2])  11.4 us
  transfers between devices with their start and end apart: 16, of which 11 were waited for; matrix products, arithmetic and copies ran while one was open for 7% of the time, Pallas kernels for 0%

profile of v3, /device:TPU:1, one launch (start us, length us, event | category | flops | bytes accessed | tf_op | source)
XLA Modules:
  0.0 259.9 jit_solution(8812538090652639350)
XLA Ops:
  6.6 1.9 shard_map.172
  8.5 11.4 %all_to_all.35 = bf16[4,32,1664]{2,1,0:T(8,128)(2,1)S(1)} all-to-all(bf16[4,32,1664]{2,1,0:T(8,128)(2,1)} %get-tuple-element.21), channel_id=1, replica_groups=mesh['z'=16,'y'=4,'x'=4,'c'=2] {'y'}, dimensions={0} | all-to-all | bytes 851968 | tf_op jit(solution)/shard_map/all_to_all | solution.py:353
  21.6 41.8 %all_gather.6 = bf16[512,896]{1,0:T(8,128)(2,1)S(1)} all-gather(bf16[32,896]{1,0:T(8,128)(2,1)} %get-tuple-element.23), channel_id=1, replica_groups=mesh['z'=16,'y'=4,'x'=4,'c'=2] {'z'}, dimensions={0}, use_global_device_ids=true | all-gather | bytes 974848 | tf_op jit(solution)/shard_map/all_gather | solution.py:356
  63.4 2.2 collective-permute-start.1
  65.6 4.3 %collective-permute-start.3 = (bf16[512,896]{1,0:T(8,128)(2,1)S(1)}, bf16[512,896]{1,0:T(8,128)(2,1)S(1)}, u32[]{:S(2)}, u32[]{:S(2)}) collective-permute-start(bf16[512,896]{1,0:T(8,128)(2,1)S(1)} %all_gather.6), channel_id=1, source_target_pairs={{0,24},{8,0},{16,8},{24,16},{1,25},{9,1},{17,9},{25,17},{2,26},{10... | collective-permute-start | bytes 2752520 | tf_op jit(solution)/shard_map/ppermute | solution.py:38
  72.0 11.3 %all_to_all.36 = bf16[4,32,2048]{2,1,0:T(8,128)(2,1)S(1)} all-to-all(bf16[4,32,2048]{2,1,0:T(8,128)(2,1)S(1)} %broadcast_in_dim.30), channel_id=1, replica_groups=mesh['z'=16,'y'=4,'x'=4,'c'=2] {'x'}, dimensions={0} | all-to-all | bytes 1048576 | tf_op jit(solution)/shard_map/all_to_all | solution.py:29
  83.3 12.1 %collective-permute-start = (bf16[128,2048]{1,0:T(8,128)(2,1)S(1)}, bf16[128,2048]{1,0:T(8,128)(2,1)S(1)}, u32[]{:S(2)}, u32[]{:S(2)}) collective-permute-start(bf16[128,2048]{1,0:T(8,128)(2,1)S(1)} %bitcast.36), channel_id=1, source_target_pairs={{0,1},{1,0},{2,3},{3,2},{4,5},{5,4},{6,7},{7,6},{8,9},{9,8},{10,11... | collective-permute-start | bytes 1572872 | tf_op jit(solution)/shard_map/ppermute | solution.py:33
  99.0 4.6 %collective-permute-start.4 = (bf16[256,896]{1,0:T(8,128)(2,1)}, bf16[256,896]{1,0:T(8,128)(2,1)}, u32[]{:S(2)}, u32[]{:S(2)}) collective-permute-start(bf16[256,896]{1,0:T(8,128)(2,1)} %slice.13), channel_id=1, source_target_pairs={{0,24},{8,0},{16,8},{24,16},{1,25},{9,1},{17,9},{25,17},{2,26},{10... | collective-permute-start | bytes 1376264 | tf_op jit(solution)/shard_map/ppermute | solution.py:38
  104.9 2.2 broadcast_in_dim.32
  108.1 3.6 %collective-permute-done.2 = bf16[256,896]{1,0:T(8,128)(2,1)} collective-permute-done((bf16[256,896]{1,0:T(8,128)(2,1)}, bf16[256,896]{1,0:T(8,128)(2,1)}, u32[]{:S(2)}, u32[]{:S(2)}) %collective-permute-start.2) | collective-permute-done | bytes 458784 | tf_op jit(solution)/shard_map/ppermute | solution.py:38
  116.7 4.3 %all-gather.2.cloned.1.call-done.gate_up_ref.gate_up = bf16[2048,1664]{1,0:T(8,128)(2,1)} async-done(((bf16[128,1664]{1,0:T(8,128)(2,1)}), bf16[2048,1664]{1,0:T(8,128)(2,1)}) %all-gather.2.cloned.1.call-update) | async-done | bytes 6815760 | tf_op jit(solution)/shard_map/all_gather | solution.py:355
  121.1 9.2 %shard_map.173 = (bf16[128,2048]{1,0:T(8,128)(2,1)}, bf16[128,2048]{1,0:T(8,128)(2,1)}) custom-call(bf16[128,2048]{1,0:T(8,128)(2,1)} %bitcast.37, bf16[128,2048]{1,0:T(8,128)(2,1)} %copy-done.7, bf16[2048,1664]{1,0:T(8,128)(2,1)} %all-gather.2.cloned.1.call-done.gate_up_ref.gate_up, bf16[2048,896]{1,0:T(8,128)(2,1)} %bitcast.15.down_ref.down, ...), custom_call_target="tpu_custom_call" | custom-call | flops 2415919104 | bytes 11534336 | tf_op jit(solution)/shard_map/pallas_call | solution.py:194
  130.3 3.1 %collective-permute-start.5 = (bf16[128,2048]{1,0:T(8,128)(2,1)}, bf16[128,2048]{1,0:T(8,128)(2,1)S(1)}, u32[]{:S(2)}, u32[]{:S(2)}) collective-permute-start(bf16[128,2048]{1,0:T(8,128)(2,1)} %get-tuple-element.28), channel_id=1, source_target_pairs={{0,1},{1,0},{2,3},{3,2},{4,5},{5,4},{6,7},{7,6},{8,9},{9,8},{10,11... | collective-permute-start | bytes 1572872 | tf_op jit(solution)/shard_map/ppermute | solution.py:33
  133.4 2.3 slice.14
  135.7 3.1 %collective-permute-start.7 = (bf16[2048,256]{1,0:T(8,128)(2,1)}, bf16[2048,256]{1,0:T(8,128)(2,1)}, u32[]{:S(2)}, u32[]{:S(2)}) collective-permute-start(bf16[2048,256]{1,0:T(8,128)(2,1)} %slice.14), channel_id=1, source_target_pairs={{0,8},{8,16},{16,24},{24,0},{1,9},{9,17},{17,25},{25,1},{2,10},{10... | collective-permute-start | bytes 3145736 | tf_op jit(solution)/shard_map/ppermute | solution.py:38
  138.8 2.0 add_convert_fusion.2
  140.8 4.0 %all-to-all-start.2 = ((bf16[4,32,2048]{2,1,0:T(8,128)(2,1)}), bf16[4,32,2048]{2,1,0:T(8,128)(2,1)S(1)}, u32[]{:S(2)}, u32[]{:S(2)}) async-start(bf16[4,32,2048]{2,1,0:T(8,128)(2,1)} %bitcast.16), calls=%async_computation.2 | async-start | bytes 1048576 | tf_op jit(solution)/shard_map/all_to_all | solution.py:128
  144.7 3.4 %collective-permute-start.8 = (bf16[2048,256]{1,0:T(8,128)(2,1)}, bf16[2048,256]{1,0:T(8,128)(2,1)}, u32[]{:S(2)}, u32[]{:S(2)}) collective-permute-start(bf16[2048,256]{1,0:T(8,128)(2,1)} %slice.14), channel_id=1, source_target_pairs={{0,24},{8,0},{16,8},{24,16},{1,25},{9,1},{17,9},{25,17},{2,26},{10... | collective-permute-start | bytes 3145736 | tf_op jit(solution)/shard_map/ppermute | solution.py:38
  148.1 5.6 %all-to-all-done.2 = bf16[4,32,2048]{2,1,0:T(8,128)(2,1)S(1)} async-done(((bf16[4,32,2048]{2,1,0:T(8,128)(2,1)}), bf16[4,32,2048]{2,1,0:T(8,128)(2,1)S(1)}, u32[]{:S(2)}, u32[]{:S(2)}) %all-to-all-start.2) | async-done | bytes 524320 | tf_op jit(solution)/shard_map/all_to_all | solution.py:128
  154.0 9.8 %collective-permute-done.7 = bf16[2048,256]{1,0:T(8,128)(2,1)} collective-permute-done((bf16[2048,256]{1,0:T(8,128)(2,1)}, bf16[2048,256]{1,0:T(8,128)(2,1)}, u32[]{:S(2)}, u32[]{:S(2)}) %collective-permute-start.7) | collective-permute-done | bytes 1048608 | tf_op jit(solution)/shard_map/ppermute | solution.py:38
  166.7 4.2 %all-to-all-start.3 = ((bf16[4,32,2048]{2,1,0:T(8,128)(2,1)}), bf16[4,32,2048]{2,1,0:T(8,128)(2,1)S(1)}, u32[]{:S(2)}, u32[]{:S(2)}) async-start(bf16[4,32,2048]{2,1,0:T(8,128)(2,1)} %broadcast_in_dim.35), calls=%async_computation.3 | async-start | bytes 1048576 | tf_op jit(solution)/shard_map/all_to_all | solution.py:29
  171.0 7.8 %all-to-all-done.3 = bf16[4,32,2048]{2,1,0:T(8,128)(2,1)S(1)} async-done(((bf16[4,32,2048]{2,1,0:T(8,128)(2,1)}), bf16[4,32,2048]{2,1,0:T(8,128)(2,1)S(1)}, u32[]{:S(2)}, u32[]{:S(2)}) %all-to-all-start.3) | async-done | bytes 524320 | tf_op jit(solution)/shard_map/all_to_all | solution.py:29
  178.8 4.5 %collective-permute-start.6 = (bf16[128,2048]{1,0:T(8,128)(2,1)S(1)}, bf16[128,2048]{1,0:T(8,128)(2,1)S(1)}, u32[]{:S(2)}, u32[]{:S(2)}) collective-permute-start(bf16[128,2048]{1,0:T(8,128)(2,1)S(1)} %bitcast.30), channel_id=1, source_target_pairs={{0,1},{1,0},{2,3},{3,2},{4,5},{5,4},{6,7},{7,6},{8,9},{9,8},{10,11... | collective-permute-start | bytes 1572872 | tf_op jit(solution)/shard_map/ppermute | solution.py:33
  184.8 6.3 %collective-permute-done.9 = bf16[2048,256]{1,0:T(8,128)(2,1)} collective-permute-done((bf16[2048,256]{1,0:T(8,128)(2,1)}, bf16[2048,256]{1,0:T(8,128)(2,1)}, u32[]{:S(2)}, u32[]{:S(2)}) %collective-permute-start.9) | collective-permute-done | bytes 1048608 | tf_op jit(solution)/shard_map/ppermute | solution.py:38
  191.2 6.2 %shard_map.174 = (bf16[128,2048]{1,0:T(8,128)(2,1)S(1)}, bf16[128,2048]{1,0:T(8,128)(2,1)S(1)}) custom-call(s32[2]{0:T(128)S(1)} %pad_add_fusion.place_ref, bf16[128,2048]{1,0:T(8,128)(2,1)S(1)} %bitcast.31, bf16[128,2048]{1,0:T(8,128)(2,1)S(1)} %collective-permute-done.6.far_ref, bf16[16,4,32,256]{3,2,1,0:T(8,128)(2,1)} %bitcast.18.own_ref, ...), custom_call_target="tpu_custom_call" | custom-call | flops 1342177280 | bytes 6291456 | tf_op jit(solution)/shard_map/pallas_call | solution.py:303
  197.4 3.6 %collective-permute-start.10 = (bf16[128,2048]{1,0:T(8,128)(2,1)S(1)}, bf16[128,2048]{1,0:T(8,128)(2,1)S(1)}, u32[]{:S(2)}, u32[]{:S(2)}) collective-permute-start(bf16[128,2048]{1,0:T(8,128)(2,1)S(1)} %get-tuple-element.32), channel_id=1, source_target_pairs={{0,1},{1,0},{2,3},{3,2},{4,5},{5,4},{6,7},{7,6},{8,9},{9,8},{10,11... | collective-permute-start | bytes 1572872 | tf_op jit(solution)/shard_map/ppermute | solution.py:33
  202.7 12.4 %all_to_all.37 = bf16[4,32,2048]{2,1,0:T(8,128)(2,1)S(1)} all-to-all(bf16[4,32,2048]{2,1,0:T(8,128)(2,1)S(1)} %bitcast.38), channel_id=1, replica_groups=mesh['z'=16,'y'=4,'x'=4,'c'=2] {'x'}, dimensions={0} | all-to-all | bytes 1048576 | tf_op jit(solution)/shard_map/all_to_all | solution.py:128
  215.5 10.2 %all_to_all.38 = bf16[4,32,2048]{2,1,0:T(8,128)(2,1)S(1)} all-to-all(bf16[4,32,2048]{2,1,0:T(8,128)(2,1)S(1)} %broadcast_in_dim.40), channel_id=1, replica_groups=mesh['z'=16,'y'=4,'x'=4,'c'=2] {'x'}, dimensions={0} | all-to-all | bytes 1048576 | tf_op jit(solution)/shard_map/all_to_all | solution.py:29
  225.7 4.7 %collective-permute-start.11 = (bf16[128,2048]{1,0:T(8,128)(2,1)S(1)}, bf16[128,2048]{1,0:T(8,128)(2,1)S(1)}, u32[]{:S(2)}, u32[]{:S(2)}) collective-permute-start(bf16[128,2048]{1,0:T(8,128)(2,1)S(1)} %bitcast.32), channel_id=1, source_target_pairs={{0,1},{1,0},{2,3},{3,2},{4,5},{5,4},{6,7},{7,6},{8,9},{9,8},{10,11... | collective-permute-start | bytes 1572872 | tf_op jit(solution)/shard_map/ppermute | solution.py:33
  231.8 4.9 %shard_map.175 = (bf16[128,2048]{1,0:T(8,128)(2,1)S(1)}, bf16[128,2048]{1,0:T(8,128)(2,1)S(1)}) custom-call(bf16[128,2048]{1,0:T(8,128)(2,1)S(1)} %bitcast.33, bf16[128,2048]{1,0:T(8,128)(2,1)S(1)} %collective-permute-done.11.far_ref, bf16[2048,1664]{1,0:T(8,128)(2,1)S(1)} %bitcast.29, bf16[2048,896]{1,0:T(8,128)(2,1)} %bitcast.15.down_ref.down, ...), custom_call_target="tpu_custom_call" | custom-call | flops 2415919104 | bytes 11534336 | tf_op jit(solution)/shard_map/pallas_call | solution.py:194
  236.7 2.3 collective-permute-start.12
  240.7 11.6 %all_to_all.39 = bf16[4,32,2048]{2,1,0:T(8,128)(2,1)S(1)} all-to-all(bf16[4,32,2048]{2,1,0:T(8,128)(2,1)S(1)} %bitcast.39), channel_id=1, replica_groups=mesh['z'=16,'y'=4,'x'=4,'c'=2] {'x'}, dimensions={0} | all-to-all | bytes 1048576 | tf_op jit(solution)/shard_map/all_to_all | solution.py:128
  (86 shorter events, 25.3 us)
Async XLA Ops:
  6.5 97.1 %copy-start.10 = (f32[768]{0:T(1024)S(1)}, f32[768]{0:T(1024)}, u32[]{:S(2)}) copy-start(f32[768]{0:T(1024)} %param.23) | copy-start | bytes 9220
  6.5 97.6 %copy-start.11 = (f32[768]{0:T(1024)S(1)}, f32[768]{0:T(1024)}, u32[]{:S(2)}) copy-start(f32[768]{0:T(1024)} %param.25) | copy-start | bytes 9220
  6.5 98.3 %copy-start.14 = (f32[256]{0:T(256)S(1)}, f32[256]{0:T(256)}, u32[]{:S(2)}) copy-start(f32[256]{0:T(256)} %param.29) | copy-start | bytes 3076
  6.5 98.3 %copy-start.13 = (f32[256]{0:T(256)S(1)}, f32[256]{0:T(256)}, u32[]{:S(2)}) copy-start(f32[256]{0:T(256)} %param.31) | copy-start | bytes 3076
  6.5 98.3 %copy-start.12 = (f32[256]{0:T(256)S(1)}, f32[256]{0:T(256)}, u32[]{:S(2)}) copy-start(f32[256]{0:T(256)} %param.33) | copy-start | bytes 3076
  6.5 114.5 %all-gather.2.cloned.1.call-start = ((), (), s32[]{:S(2)}) async-start(), calls=%async_computation.7 | async-start | bytes 7241728 | tf_op jit(solution)/shard_map/all_gather | solution.py:355
  63.4 32.0 %collective-permute-start.1 = (bf16[512,896]{1,0:T(8,128)(2,1)S(1)}, bf16[512,896]{1,0:T(8,128)(2,1)S(1)}, u32[]{:S(2)}, u32[]{:S(2)}) collective-permute-start(bf16[512,896]{1,0:T(8,128)(2,1)S(1)} %all_gather.6), channel_id=1, source_target_pairs={{0,8},{8,16},{16,24},{24,0},{1,9},{9,17},{17,25},{25,1},{2,10},{10... | collective-permute-start | bytes 2752520 | tf_op jit(solution)/shard_map/ppermute | solution.py:38
  65.6 32.5 %collective-permute-start.3 = (bf16[512,896]{1,0:T(8,128)(2,1)S(1)}, bf16[512,896]{1,0:T(8,128)(2,1)S(1)}, u32[]{:S(2)}, u32[]{:S(2)}) collective-permute-start(bf16[512,896]{1,0:T(8,128)(2,1)S(1)} %all_gather.6), channel_id=1, source_target_pairs={{0,24},{8,0},{16,8},{24,16},{1,25},{9,1},{17,9},{25,17},{2,26},{10... | collective-permute-start | bytes 2752520 | tf_op jit(solution)/shard_map/ppermute | solution.py:38
  83.3 24.9 %copy-start.2 = (bf16[4,32,2048]{2,1,0:T(8,128)(2,1)}, bf16[4,32,2048]{2,1,0:T(8,128)(2,1)S(1)}, u32[]{:S(2)}) copy-start(bf16[4,32,2048]{2,1,0:T(8,128)(2,1)S(1)} %all_to_all.36) | copy-start | bytes 1572868
  83.3 21.6 %collective-permute-start = (bf16[128,2048]{1,0:T(8,128)(2,1)S(1)}, bf16[128,2048]{1,0:T(8,128)(2,1)S(1)}, u32[]{:S(2)}, u32[]{:S(2)}) collective-permute-start(bf16[128,2048]{1,0:T(8,128)(2,1)S(1)} %bitcast.36), channel_id=1, source_target_pairs={{0,1},{1,0},{2,3},{3,2},{4,5},{5,4},{6,7},{7,6},{8,9},{9,8},{10,11... | collective-permute-start | bytes 1572872 | tf_op jit(solution)/shard_map/ppermute | solution.py:33
  95.3 2.8 %copy-start.3 = (bf16[512,896]{1,0:T(8,128)(2,1)}, bf16[512,896]{1,0:T(8,128)(2,1)S(1)}, u32[]{:S(2)}) copy-start(bf16[512,896]{1,0:T(8,128)(2,1)S(1)} %collective-permute-done.1) | copy-start | bytes 2752516
  96.2 15.5 %collective-permute-start.2 = (bf16[256,896]{1,0:T(8,128)(2,1)}, bf16[256,896]{1,0:T(8,128)(2,1)}, u32[]{:S(2)}, u32[]{:S(2)}) collective-permute-start(bf16[256,896]{1,0:T(8,128)(2,1)} %slice.12), channel_id=1, source_target_pairs={{0,8},{8,16},{16,24},{24,0},{1,9},{9,17},{17,25},{25,1},{2,10},{10... | collective-permute-start | bytes 1376264 | tf_op jit(solution)/shard_map/ppermute | solution.py:38
  99.0 14.4 %collective-permute-start.4 = (bf16[256,896]{1,0:T(8,128)(2,1)}, bf16[256,896]{1,0:T(8,128)(2,1)}, u32[]{:S(2)}, u32[]{:S(2)}) collective-permute-start(bf16[256,896]{1,0:T(8,128)(2,1)} %slice.13), channel_id=1, source_target_pairs={{0,24},{8,0},{16,8},{24,16},{1,25},{9,1},{17,9},{25,17},{2,26},{10... | collective-permute-start | bytes 1376264 | tf_op jit(solution)/shard_map/ppermute | solution.py:38
  104.8 2.3 copy-start.4
  104.9 9.8 %copy-start.7 = (bf16[128,2048]{1,0:T(8,128)(2,1)}, bf16[128,2048]{1,0:T(8,128)(2,1)S(1)}, u32[]{:S(2)}) copy-start(bf16[128,2048]{1,0:T(8,128)(2,1)S(1)} %collective-permute-done.far_ref) | copy-start | bytes 1572868
  130.3 23.6 %copy-start.6 = (bf16[32,2048]{1,0:T(8,128)(2,1)S(1)}, bf16[32,2048]{1,0:T(8,128)(2,1)}, u32[]{:S(2)}) copy-start(bf16[32,2048]{1,0:T(8,128)(2,1)} %param.18) | copy-start | bytes 393220
  130.3 35.4 %copy-start.8 = (f32[2048]{0:T(1024)S(1)}, f32[2048]{0:T(1024)}, u32[]{:S(2)}) copy-start(f32[2048]{0:T(1024)} %param.20) | copy-start | bytes 24580
  130.3 8.5 %collective-permute-start.5 = (bf16[128,2048]{1,0:T(8,128)(2,1)}, bf16[128,2048]{1,0:T(8,128)(2,1)S(1)}, u32[]{:S(2)}, u32[]{:S(2)}) collective-permute-start(bf16[128,2048]{1,0:T(8,128)(2,1)} %get-tuple-element.28), channel_id=1, source_target_pairs={{0,1},{1,0},{2,3},{3,2},{4,5},{5,4},{6,7},{7,6},{8,9},{9,8},{10,11... | collective-permute-start | bytes 1572872 | tf_op jit(solution)/shard_map/ppermute | solution.py:33
  135.7 28.1 %collective-permute-start.7 = (bf16[2048,256]{1,0:T(8,128)(2,1)}, bf16[2048,256]{1,0:T(8,128)(2,1)}, u32[]{:S(2)}, u32[]{:S(2)}) collective-permute-start(bf16[2048,256]{1,0:T(8,128)(2,1)} %slice.14), channel_id=1, source_target_pairs={{0,8},{8,16},{16,24},{24,0},{1,9},{9,17},{17,25},{25,1},{2,10},{10... | collective-permute-start | bytes 3145736 | tf_op jit(solution)/shard_map/ppermute | solution.py:38
  140.8 13.0 %all-to-all-start.2 = ((bf16[4,32,2048]{2,1,0:T(8,128)(2,1)}), bf16[4,32,2048]{2,1,0:T(8,128)(2,1)S(1)}, u32[]{:S(2)}, u32[]{:S(2)}) async-start(bf16[4,32,2048]{2,1,0:T(8,128)(2,1)} %bitcast.16), calls=%async_computation.2 | async-start | bytes 1048576 | tf_op jit(solution)/shard_map/all_to_all | solution.py:128
  144.7 39.1 %collective-permute-start.8 = (bf16[2048,256]{1,0:T(8,128)(2,1)}, bf16[2048,256]{1,0:T(8,128)(2,1)}, u32[]{:S(2)}, u32[]{:S(2)}) collective-permute-start(bf16[2048,256]{1,0:T(8,128)(2,1)} %slice.14), channel_id=1, source_target_pairs={{0,24},{8,0},{16,8},{24,16},{1,25},{9,1},{17,9},{25,17},{2,26},{10... | collective-permute-start | bytes 3145736 | tf_op jit(solution)/shard_map/ppermute | solution.py:38
  163.8 27.3 %collective-permute-start.9 = (bf16[2048,256]{1,0:T(8,128)(2,1)}, bf16[2048,256]{1,0:T(8,128)(2,1)}, u32[]{:S(2)}, u32[]{:S(2)}) collective-permute-start(bf16[2048,256]{1,0:T(8,128)(2,1)} %collective-permute-done.7), channel_id=1, source_target_pairs={{0,8},{8,16},{16,24},{24,0},{1,9},{9,17},{17,25},{25,1},{2,10},{10... | collective-permute-start | bytes 3145736 | tf_op jit(solution)/shard_map/ppermute | solution.py:38
  166.7 65.1 %slice-start = ((s8[6815744]{0:T(1024)(128)(4,1)}), s8[2621440]{0:T(1024)(128)(4,1)S(1)}, s32[]{:S(2)}) async-start(s8[6815744]{0:T(1024)(128)(4,1)} %bitcast.28), calls=%async_computation.8 | async-start | bytes 5242880
  166.7 12.1 %all-to-all-start.3 = ((bf16[4,32,2048]{2,1,0:T(8,128)(2,1)}), bf16[4,32,2048]{2,1,0:T(8,128)(2,1)S(1)}, u32[]{:S(2)}, u32[]{:S(2)}) async-start(bf16[4,32,2048]{2,1,0:T(8,128)(2,1)} %broadcast_in_dim.35), calls=%async_computation.3 | async-start | bytes 1048576 | tf_op jit(solution)/shard_map/all_to_all | solution.py:29
  178.8 6.0 %collective-permute-start.6 = (bf16[128,2048]{1,0:T(8,128)(2,1)S(1)}, bf16[128,2048]{1,0:T(8,128)(2,1)S(1)}, u32[]{:S(2)}, u32[]{:S(2)}) collective-permute-start(bf16[128,2048]{1,0:T(8,128)(2,1)S(1)} %bitcast.30), channel_id=1, source_target_pairs={{0,1},{1,0},{2,3},{3,2},{4,5},{5,4},{6,7},{7,6},{8,9},{9,8},{10,11... | collective-permute-start | bytes 1572872 | tf_op jit(solution)/shard_map/ppermute | solution.py:33
  191.2 24.2 %copy-start.9 = (f32[2048]{0:T(1024)S(1)}, f32[2048]{0:T(1024)}, u32[]{:S(2)}) copy-start(f32[2048]{0:T(1024)} %param.21) | copy-start | bytes 24580
  191.2 40.6 %slice-start.1 = ((s8[6815744]{0:T(1024)(128)(4,1)}), s8[4194304]{0:T(1024)(128)(4,1)S(1)}, s32[]{:S(2)}) async-start(s8[6815744]{0:T(1024)(128)(4,1)} %bitcast.28), calls=%async_computation.9 | async-start | bytes 8388608
  197.4 34.4 %copy-start = (f32[1,768]{1,0:T(1,128)S(1)}, f32[1,768]{1,0:T(1,128)}, u32[]{:S(2)}) copy-start(f32[1,768]{1,0:T(1,128)} %broadcast_in_dim.33.gate_scale) | copy-start | bytes 9220
  197.4 34.4 %copy-start.1 = (f32[1,768]{1,0:T(1,128)S(1)}, f32[1,768]{1,0:T(1,128)}, u32[]{:S(2)}) copy-start(f32[1,768]{1,0:T(1,128)} %broadcast_in_dim.34.up_scale) | copy-start | bytes 9220
  197.4 5.1 %collective-permute-start.10 = (bf16[128,2048]{1,0:T(8,128)(2,1)S(1)}, bf16[128,2048]{1,0:T(8,128)(2,1)S(1)}, u32[]{:S(2)}, u32[]{:S(2)}) collective-permute-start(bf16[128,2048]{1,0:T(8,128)(2,1)S(1)} %get-tuple-element.32), channel_id=1, source_target_pairs={{0,1},{1,0},{2,3},{3,2},{4,5},{5,4},{6,7},{7,6},{8,9},{9,8},{10,11... | collective-permute-start | bytes 1572872 | tf_op jit(solution)/shard_map/ppermute | solution.py:33
  225.7 6.1 %collective-permute-start.11 = (bf16[128,2048]{1,0:T(8,128)(2,1)S(1)}, bf16[128,2048]{1,0:T(8,128)(2,1)S(1)}, u32[]{:S(2)}, u32[]{:S(2)}) collective-permute-start(bf16[128,2048]{1,0:T(8,128)(2,1)S(1)} %bitcast.32), channel_id=1, source_target_pairs={{0,1},{1,0},{2,3},{3,2},{4,5},{5,4},{6,7},{7,6},{8,9},{9,8},{10,11... | collective-permute-start | bytes 1572872 | tf_op jit(solution)/shard_map/ppermute | solution.py:33
  236.7 3.8 %collective-permute-start.12 = (bf16[128,2048]{1,0:T(8,128)(2,1)S(1)}, bf16[128,2048]{1,0:T(8,128)(2,1)S(1)}, u32[]{:S(2)}, u32[]{:S(2)}) collective-permute-start(bf16[128,2048]{1,0:T(8,128)(2,1)S(1)} %get-tuple-element.34), channel_id=1, source_target_pairs={{0,1},{1,0},{2,3},{3,2},{4,5},{5,4},{6,7},{7,6},{8,9},{9,8},{10,11... | collective-permute-start | bytes 1572872 | tf_op jit(solution)/shard_map/ppermute | solution.py:33
  (1 other events, 0.8 us)
Sparse Core Ops, SparseCore 0:
  21.7 99.3 all-gather.1
